TPU v7x, 256 devices: a 4x2x16 block of a 4x16x16 slice. The times are simulated.
256 devices in a mesh: grp: 2 (over y), ep: 32 (over z, core), tp: 4 (over x).
Axes of the slice: x: 4, y: 2, z: 16, core: 2. Of those that a mesh axis runs over, the one named last changes fastest.
The devices are a block of a 4x16x16 slice.
Arguments:
- query_vectors: bfloat16 [32768, 2048], P(('grp', 'ep'), 'tp'), parts along dimension 0, may hold values from -6 to 6
- attend_lookup_vectors: bfloat16 [32768, 2048], P(('grp', 'ep'), 'tp'), parts along dimension 0, may hold values from -6 to 6
- attend_content_vectors: bfloat16 [32768, 2048], P(('grp', 'ep'), 'tp'), parts along dimension 0, may hold values from -6 to 6
- forget_speed_dependent: bfloat16 [32768, 2048], P(('grp', 'ep'), 'tp'), parts along dimension 0, may hold values from -3 to 3
- amend_speed_dependent: bfloat16 [32768, 2048], P(('grp', 'ep'), 'tp'), parts along dimension 0, may hold values from -6 to 6
- result_switch_preactivation: bfloat16 [32768, 2048], P(('grp', 'ep'), 'tp'), parts along dimension 0, may hold values from -6 to 6
- feature_forget_baseline: float32 [2048], P('tp'), may hold values from -13 to -3
- amend_speed_baseline: float32 [2048], P('tp'), may hold values from -9 to 3
- sudden_forget_extra: float32 [32768, 32], P(('grp', 'ep'), 'tp'), parts along dimension 0, may hold values from -1 to 0
- group_scaling_factor: float32 [2048], P('tp'), may hold values from 0.1 to 1.9
- result_mapping_matrix: bfloat16 [2048, 2048], P('tp'), may hold values from -0.125 to 0.125
- specialist_tokens_activations: bfloat16 [32768, 2048], P(('grp', 'ep', 'tp')), parts along dimension 0, may hold values from -6 to 6
- specialist_scaling_factor: float32 [2048], replicated, may hold values from 0.1 to 1.9
- selected_specialists: int32 [32768, 2], P(('grp', 'ep', 'tp')), parts along dimension 0, may hold values from 0 to 31, all different within a row; in each aligned block of 128 rows (0 to 127, 128 to 255, ...) at most 12 rows name the same one
- selection_mixing_factors: float32 [32768, 2], P(('grp', 'ep', 'tp')), parts along dimension 0, may hold values from 0.3 to 1.5
- dispatched_switch_matrix: bfloat16 [32, 2048, 1024], P('ep', None, 'tp'), may hold values from -0.125 to 0.125
- dispatched_raising_matrix: bfloat16 [32, 2048, 1024], P('ep', None, 'tp'), may hold values from -0.125 to 0.125
- dispatched_lowering_matrix: bfloat16 [32, 1024, 2048], P('ep', 'tp'), may hold values from -0.1875 to 0.1875
- common_switch_matrix: bfloat16 [2048, 512], P(None, 'tp'), may hold values from -0.125 to 0.125
- common_raising_matrix: bfloat16 [2048, 512], P(None, 'tp'), may hold values from -0.125 to 0.125
- common_lowering_matrix: bfloat16 [512, 2048], P('tp'), may hold values from -0.25 to 0.25
Outputs:
- attend_result_matrix: bfloat16 [32768, 2048], P(('grp', 'ep', 'tp')), parts along dimension 0
- moe_out: bfloat16 [32768, 2048], P(('grp', 'ep', 'tp')), parts along dimension 0
There are 2 independent parts, one for each index of `grp`. A program takes and returns all parts, laid end to end along the dimension named above; an argument that names none is the same for every part. Nothing has to cross between parts.
Inputs may be any that keep to these rules, and one draw needn't show every extreme that they name: `selected_specialists`: each row names 2 different experts. Among the rows of one device no expert is named more than 12 times, and in every draw some device names some expert exactly 12 times.
All inputs are finite; a program needn't handle non-finite values.
Results may differ from a plain program's by a relative error of at most 0.023.
Values may be sent and summed in bfloat16 or wider, within the bound.
No kernel may reach another device: no remote copies, remote signals or barrier semaphores. Data moves between devices by JAX's collectives and lax.ppermute only.
A program may use at most 128 MiB of HBM per device.

v0:
```python
import jax
import jax.numpy as jnp
from jax import lax
from jax.experimental import pallas as pl
from jax.experimental.pallas import tpu as pltpu
from jax.sharding import PartitionSpec as P


F32 = jnp.float32
BF16 = jnp.bfloat16
SPAN = 64
VMEM_LIMIT = 56 * 1024 * 1024


def mm(a, b):
    return lax.dot_general(a, b, (((1,), (0,)), ((), ())), preferred_element_type=F32)


def mm_nt(a, b):
    return lax.dot_general(a, b, (((1,), (1,)), ((), ())), preferred_element_type=F32)


def mm_tn(a, b):
    return lax.dot_general(a, b, (((0,), (0,)), ((), ())), preferred_element_type=F32)


def iota(shape, dim):
    return lax.broadcasted_iota(jnp.int32, shape, dim)


def split_two(x):
    hi = x.astype(BF16)
    lo = (x - hi.astype(F32)).astype(BF16)
    return hi, lo


def sigmoid(x):
    return 1.0 / (1.0 + jnp.exp(-x))


def mixer_local(q_ref, k_ref, v_ref, f_ref, a_ref, x_ref, fb_ref, ab_ref, out_ref, q2_ref, ex_ref, state_ref):
    tokens, width = q_ref.shape
    half = width // 2
    spans = tokens // SPAN
    pair = pl.program_id(0)
    lane = iota((SPAN, width), 1)
    row = iota((SPAN, width), 0)
    first = lane < half
    col = lane % half
    strict = row > col
    inclusive = row >= col
    eye = (row == col).astype(F32)
    tril = (iota((SPAN, SPAN), 0) >= iota((SPAN, SPAN), 1)).astype(BF16)
    ones_bd = ((iota((2 * width, width), 0) % width) // half == iota((2 * width, width), 1) // half).astype(BF16)
    levels = []
    size = 1
    while size < SPAN:
        levels.append(
            (row // (2 * size) == col // (2 * size)) & (row % (2 * size) >= size) & (col % (2 * size) < size)
        )
        size *= 2

    def bd(x):
        zero = jnp.zeros_like(x)
        return jnp.concatenate([jnp.where(first, x, zero), jnp.where(first, zero, x)], axis=0)

    heads = x_ref.shape[1]
    head_lane = iota((SPAN, heads), 1)
    fb = fb_ref[...]
    ab = ab_ref[...]

    def prepare(c):
        rows = pl.ds(pl.multiple_of(c * SPAN, SPAN), SPAN)
        extra = x_ref[rows, :]
        extra_a = jnp.sum(jnp.where(head_lane == 2 * pair, extra, 0.0), axis=1, keepdims=True)
        extra_b = jnp.sum(jnp.where(head_lane == 2 * pair + 1, extra, 0.0), axis=1, keepdims=True)
        decay = jnp.where(first, extra_a, extra_b) - jnp.exp(fb + f_ref[rows, :].astype(F32))
        hi = decay.astype(BF16)
        rest = decay - hi.astype(F32)
        mid = rest.astype(BF16)
        low = (rest - mid.astype(F32)).astype(BF16)
        sums = mm(tril, jnp.concatenate([hi, mid, low], axis=1))
        cum = sums[:, :width] + sums[:, width : 2 * width] + sums[:, 2 * width :]
        key = k_ref[rows, :].astype(F32)
        sq_hi, sq_lo = split_two(key * key)
        total = mm(jnp.concatenate([sq_hi, sq_lo], axis=1), ones_bd) + 1e-06
        inv = lax.rsqrt(total)
        unit = key * inv
        erase = unit * sigmoid(ab + a_ref[rows, :].astype(F32))
        scaled_value = v_ref[rows, :].astype(F32) * (total * inv)
        center = cum[SPAN // 2 : SPAN // 2 + 1, :]
        last = cum[SPAN - 1 : SPAN, :]
        left_erase = -unit * jnp.exp(cum - decay - center)
        left_read = q_ref[rows, :].astype(F32) * jnp.exp(cum - center)
        right = erase * jnp.exp(center - cum)
        pairs = mm_nt(jnp.concatenate([left_erase, left_read], axis=0).astype(BF16), bd(right.astype(BF16)))
        lower = jnp.where(strict, pairs[:SPAN], 0.0)
        read = jnp.where(inclusive, pairs[SPAN:], 0.0).astype(BF16)
        to_start = jnp.exp(center)
        rhs = jnp.concatenate(
            [bd(scaled_value.astype(BF16)), bd((left_erase * to_start).astype(BF16))], axis=1
        )
        read_start = left_read * to_start
        tail = (right * jnp.exp(last - center)).astype(BF16)
        return lower, read, rhs, read_start, tail, jnp.exp(last)

    state_ref[...] = jnp.concatenate([jnp.zeros((SPAN, width), F32), eye], axis=0)
    group = min(4, spans)

    @pl.loop(0, spans // group)
    def _(turn):
        start = turn * group
        state = state_ref[...]
        prepared = [prepare(start + j) for j in range(group)]
        inverse = [eye + jnp.where(levels[0], p[0], 0.0) for p in prepared]
        for level in levels[1:]:
            packed = [x.astype(BF16) for x in inverse]
            step = [
                mm(x, bd(jnp.where(level, p[0], 0.0).astype(BF16))).astype(BF16)
                for x, p in zip(packed, prepared)
            ]
            inverse = [x + mm(y, bd(xb)) for x, y, xb in zip(inverse, step, packed)]
        solved = [mm(x.astype(BF16), p[2]).astype(BF16) for x, p in zip(inverse, prepared)]
        outs = [
            mm(p[1], jnp.concatenate([bd(u[:, :width]), bd(u[:, width:])], axis=1))
            for u, p in zip(solved, prepared)
        ]
        grams = [mm_tn(u, p[4]) for u, p in zip(solved, prepared)]
        for j in range(group):
            rows = pl.ds(pl.multiple_of((start + j) * SPAN, SPAN), SPAN)
            out, gram, prep = outs[j], grams[j], prepared[j]
            reads = (out[:, width:] + prep[3]).astype(BF16)
            state_b = state.astype(BF16)
            both = mm_nt(reads, jnp.concatenate([bd(state_b[:SPAN]), bd(state_b[SPAN:])], axis=0))
            out_ref[rows, :] = out[:, :width] + both[:, :width]
            q2_ref[rows, :] = both[:, width:].astype(BF16)
            add = jnp.where(first, gram[:SPAN], gram[SPAN : 2 * SPAN])
            trans = jnp.concatenate(
                [
                    jnp.where(first, gram[2 * SPAN : 3 * SPAN], 0.0),
                    jnp.where(first, 0.0, gram[3 * SPAN :]),
                ],
                axis=0,
            ).astype(BF16)
            state = state * prep[5] + mm(state_b, trans)
            state = jnp.concatenate([state[:SPAN] + add, state[SPAN:]], axis=0)
        state_ref[...] = state

    ex_ref[...] = state_ref[...].astype(BF16)


def run_mixer_local(q, k, v, f, a, extra, fb, ab):
    tokens, width = q.shape
    heads = extra.shape[1]
    head_size = width // heads
    pairs = heads // 2
    wide = 2 * head_size
    spec = pl.BlockSpec((tokens, wide), lambda i: (0, i))
    vec = pl.BlockSpec((1, wide), lambda i: (0, i))
    return pl.pallas_call(
        mixer_local,
        grid=(pairs,),
        in_specs=[spec] * 5 + [pl.BlockSpec((tokens, heads), lambda i: (0, 0)), vec, vec],
        out_specs=[spec, spec, pl.BlockSpec((wide, wide), lambda i: (i, 0))],
        out_shape=[
            jax.ShapeDtypeStruct((tokens, width), F32),
            jax.ShapeDtypeStruct((tokens, width), BF16),
            jax.ShapeDtypeStruct((pairs * wide, wide), BF16),
        ],
        scratch_shapes=[pltpu.VMEM((2 * SPAN, wide), F32)],
        compiler_params=pltpu.CompilerParams(
            dimension_semantics=("arbitrary",), vmem_limit_bytes=VMEM_LIMIT
        ),
        cost_estimate=pl.CostEstimate(
            flops=40_000_000_000, transcendentals=2_000_000, bytes_accessed=5_000_000
        ),
        name="mixer_local",
    )(q, k, v, f, a, extra, fb.reshape(1, -1), ab.reshape(1, -1))


def chain_kernel(me_ref, r_ref, o_ref, state_ref):
    rows, wide = r_ref.shape[1:]
    half = wide // 2
    pairs = rows // wide
    first = iota((half, wide), 1) < half
    state_ref[...] = jnp.zeros_like(state_ref)

    @pl.loop(0, r_ref.shape[0])
    def _(d):
        @pl.when(d < me_ref[0])
        def _():
            for p in range(pairs):
                own = slice(p * half, (p + 1) * half)
                added = r_ref[d, p * wide : p * wide + half, :].astype(F32)
                carried = r_ref[d, p * wide + half : (p + 1) * wide, :]
                zero = jnp.zeros_like(carried)
                carried = jnp.concatenate(
                    [jnp.where(first, carried, zero), jnp.where(first, zero, carried)], axis=0
                )
                state_ref[own, :] = mm(state_ref[own, :].astype(BF16), carried) + added

    o_ref[...] = state_ref[...].astype(BF16)


def run_chain(me, gathered):
    _, rows, wide = gathered.shape
    return pl.pallas_call(
        chain_kernel,
        grid_spec=pltpu.PrefetchScalarGridSpec(
            num_scalar_prefetch=1,
            grid=(1,),
            in_specs=[pl.BlockSpec(gathered.shape, lambda i, me_ref: (0, 0, 0))],
            out_specs=pl.BlockSpec((rows // 2, wide), lambda i, me_ref: (0, 0)),
            scratch_shapes=[pltpu.VMEM((rows // 2, wide), F32)],
        ),
        out_shape=jax.ShapeDtypeStruct((rows // 2, wide), BF16),
        compiler_params=grid_params(),
        cost_estimate=pl.CostEstimate(
            flops=3_000_000_000, transcendentals=0, bytes_accessed=4_000_000
        ),
        name="chain",
    )(me, gathered)


def mixer_final(me_ref, o_ref, q2_ref, s_ref, g_ref, gain_ref, w_ref, *outs):
    width = o_ref.shape[1]
    wide = s_ref.shape[1]
    half = wide // 2
    pairs = width // wide
    first = iota((half, wide), 1) < half
    ones_bd = ((iota((2 * wide, wide), 0) % wide) // half == iota((2 * wide, wide), 1) // half).astype(BF16)

    def head_mean(x):
        hi, lo = split_two(x)
        return mm(jnp.concatenate([hi, lo], axis=1), ones_bd) * (1.0 / half)

    pieces = []
    for p in range(pairs):
        cols = slice(p * wide, (p + 1) * wide)
        state = s_ref[p * half : (p + 1) * half, :]
        zero = jnp.zeros_like(state)
        both = jnp.concatenate([jnp.where(first, state, zero), jnp.where(first, zero, state)], axis=0)
        head_out = o_ref[:, cols] + mm_nt(q2_ref[:, cols], both)
        centered = head_out - head_mean(head_out)
        var = head_mean(centered * centered)
        gate = sigmoid(g_ref[:, cols].astype(F32))
        pieces.append((centered * lax.rsqrt(var + 0.00064) * gain_ref[:, cols] * gate).astype(BF16))
    mixed = jnp.concatenate(pieces, axis=1)
    result = mm(mixed, w_ref[...]).astype(BF16)
    for d, out_ref in enumerate(outs):

        @pl.when(pl.program_id(0) == d)
        def _(out_ref=out_ref):
            out_ref[...] = result


def run_mixer_final(me, out_local, q2, starts, gate, gain, mapping, blocks):
    tokens, width = out_local.shape
    model = mapping.shape[1]
    rows = tokens // blocks

    def turned(i, me_ref):
        return ((me_ref[0] + i) % blocks, 0)

    spec = pl.BlockSpec((rows, width), turned)
    return pl.pallas_call(
        mixer_final,
        grid_spec=pltpu.PrefetchScalarGridSpec(
            num_scalar_prefetch=1,
            grid=(blocks,),
            in_specs=[
                spec,
                spec,
                pl.BlockSpec(starts.shape, lambda i, me_ref: (0, 0)),
                spec,
                pl.BlockSpec((1, width), lambda i, me_ref: (0, 0)),
                pl.BlockSpec((width, model), lambda i, me_ref: (0, 0)),
            ],
            out_specs=[pl.BlockSpec((rows, model), lambda i, me_ref: (0, 0))] * blocks,
        ),
        out_shape=[jax.ShapeDtypeStruct((rows, model), BF16)] * blocks,
        compiler_params=grid_params(),
        cost_estimate=pl.CostEstimate(
            flops=6_000_000_000, transcendentals=1_000_000, bytes_accessed=8_000_000
        ),
        name="mixer_final",
    )(me, out_local, q2, starts, gate, gain.reshape(1, -1), mapping)


def picks(size, slot_rows, cap):
    kept = size // slot_rows * cap
    r = iota((kept, 1), 0)
    block = r // cap
    s = r - block * cap
    c = iota((kept, size), 1)
    at_tail = c == block * slot_rows + cap + s // 3
    return (c == block * slot_rows + s).astype(BF16), [
        (at_tail & (s % 3 == third)).astype(BF16) for third in range(3)
    ]


def dispatch_kernel(slot_rows, cap, t_ref, scale_ref, sel_ref, normed_ref, out_ref, pos_ref):
    rows, _ = t_ref.shape
    total = out_ref.shape[0]
    main = out_ref.shape[1]
    third = main // 3
    experts = total // slot_rows
    floats = t_ref[...].astype(F32)
    mean = jnp.mean(floats * floats, axis=1, keepdims=True)
    normed = (floats * lax.rsqrt(mean + 1e-06) * scale_ref[...]).astype(BF16)
    normed_ref[...] = normed
    named = sel_ref[...].astype(F32)
    named = jnp.concatenate([named] * (8 // named.shape[0]), axis=0).T.astype(jnp.int32)
    ids = [named[:, 0:1], named[:, 1:2]]
    expert = iota((rows, experts), 1)
    hot = [(i == expert).astype(F32) for i in ids]
    strict = (iota((rows, rows), 0) > iota((rows, rows), 1)).astype(BF16)
    before = mm(strict, (hot[0] + hot[1]).astype(BF16))
    slots = [jnp.sum(h * before, axis=1, keepdims=True).astype(jnp.int32) for h in hot]
    place = iota((rows, total), 1)
    pos = [i * slot_rows + s for i, s in zip(ids, slots)]
    tail = [i * slot_rows + cap + s // 3 for i, s in zip(ids, slots)]
    which = [s % 3 for s in slots]
    pos_ref[...] = jnp.concatenate(pos, axis=1)
    main_hot = ((place == pos[0]) | (place == pos[1])).astype(BF16)
    for b in range(3):
        tail_hot = (
            ((place == tail[0]) & (which[0] == b)) | ((place == tail[1]) & (which[1] == b))
        ).astype(BF16)
        hot2 = jnp.concatenate([main_hot, tail_hot], axis=0)
        data = jnp.concatenate([normed[:, b * third : (b + 1) * third], normed[:, main:]], axis=0)
        out_ref[:, b * third : (b + 1) * third] = mm_tn(hot2, data).astype(BF16)


class Copies:
    def __init__(self, sems):
        self.sems = sems
        self.made = []

    def start(self, src, dst, group):
        copy = pltpu.make_async_copy(src, dst, self.sems.at[len(self.made)])
        copy.start()
        self.made.append((group, copy))

    def wait(self, group):
        for at, copy in self.made:
            if at == group:
                copy.wait()


def near_kernel(slot_rows, cap, r_ref, *refs):
    blocks = (len(refs) - 5) // 2
    gates, ups = refs[:blocks], refs[blocks : 2 * blocks]
    h_ref, x_ref, g_ref, u_ref, sems = refs[2 * blocks :]
    total, main = r_ref.shape
    third = main // 3
    ff = g_ref.shape[2]
    size = min(256, total)
    kept = size // slot_rows * cap
    copies = Copies(sems)
    for k in range(blocks):
        copies.start(gates[k], g_ref.at[k], k)
        copies.start(ups[k], u_ref.at[k], k)
    whole, tails = picks(size, slot_rows, cap)
    for i in range(total // size):
        rows = slice(i * kept, (i + 1) * kept)
        block = r_ref[i * size : (i + 1) * size, :]
        x_ref[rows, :main] = mm(whole, block).astype(BF16)
        acc = jnp.zeros((kept, third), F32)
        for b in range(3):
            acc = acc + mm(tails[b], block[:, b * third : (b + 1) * third])
        x_ref[rows, main:] = acc.astype(BF16)
    for k in range(blocks):
        copies.wait(k)
        gate = mm(x_ref[...], g_ref[k])
        up = mm(x_ref[...], u_ref[k])
        h_ref[:, k * ff : (k + 1) * ff] = (gate * sigmoid(gate) * up).astype(BF16)


def far_kernel(slot_rows, cap, x_hbm, h_hbm, fa, fb, *refs):
    *downs, o_ref, x_ref, h_ref, g_ref, u_ref, d_ref, tail_ref, sems = refs
    total, main = o_ref.shape
    third = main // 3
    model, ff = g_ref.shape
    near = h_ref.shape[1] - ff
    half = model // 2
    size = min(256, total)
    kept = size // slot_rows * cap
    copies = Copies(sems)
    copies.start(x_hbm, x_ref, "x")
    for src, at in ((fa, 0), (fb, half)):
        copies.start(src.at[0:half, :], g_ref.at[at : at + half, :], "x")
        copies.start(src.at[half:model, :], u_ref.at[at : at + half, :], "x")
    copies.start(h_hbm, h_ref.at[:, 0:near], "d")
    base = 0
    for src in downs:
        rows = src.shape[0]
        copies.start(src, d_ref.at[base : base + rows, :], "d")
        base += rows
    whole, tails = picks(size, slot_rows, cap)
    copies.wait("x")
    gate = mm(x_ref[...], g_ref[...])
    up = mm(x_ref[...], u_ref[...])
    copies.wait("d")
    h_ref[:, near:] = (gate * sigmoid(gate) * up).astype(BF16)
    tail_ref[...] = mm(h_ref[...], d_ref[:, main:]).astype(BF16)
    for b in range(3):
        cols = slice(b * third, (b + 1) * third)
        y = mm(h_ref[...], d_ref[:, cols]).astype(BF16)
        spread = jnp.concatenate([whole, tails[b]], axis=0)
        for i in range(total // size):
            rows = slice(i * kept, (i + 1) * kept)
            both = jnp.concatenate([y[rows], tail_ref[rows, :]], axis=0)
            o_ref[i * size : (i + 1) * size, cols] = mm_tn(spread, both).astype(BF16)


def shared_kernel(*refs):
    count = (len(refs) - 3) // 2
    rows_in, outs = refs[:count], refs[count + 3 :]
    g_ref, u_ref, d_ref = refs[count : count + 3]
    x = jnp.concatenate([ref[...] for ref in rows_in], axis=0)
    gate = mm(x, g_ref[...])
    up = mm(x, u_ref[...])
    hidden = (gate * sigmoid(gate) * up).astype(BF16)
    for d, o_ref in enumerate(outs):
        rows = o_ref.shape[0]
        o_ref[...] = mm(hidden[d * rows : (d + 1) * rows], d_ref[...]).astype(BF16)


def prepare_kernel(slot_rows, cap, pos_ref, mix_ref, *refs):
    *blocks, w_ref, base_ref = refs
    rows = pos_ref.shape[0]
    place = iota((rows, w_ref.shape[1]), 1)
    pos = [pos_ref[:, 0:1], pos_ref[:, 1:2]]
    mix = [mix_ref[:, 0:1], mix_ref[:, 1:2]]
    slots = [p % slot_rows for p in pos]
    tail = [p - s + cap + s // 3 for p, s in zip(pos, slots)]
    which = [s % 3 for s in slots]
    main = jnp.where(place == pos[0], mix[0], 0.0) + jnp.where(place == pos[1], mix[1], 0.0)
    main = main.astype(BF16)
    for b in range(3):
        w_ref[2 * b * rows : (2 * b + 1) * rows, :] = main
        w_ref[(2 * b + 1) * rows : (2 * b + 2) * rows, :] = (
            jnp.where((place == tail[0]) & (which[0] == b), mix[0], 0.0)
            + jnp.where((place == tail[1]) & (which[1] == b), mix[1], 0.0)
        ).astype(BF16)
    base = blocks[0][...].astype(F32)
    for block in blocks[1:]:
        base = base + block[...].astype(F32)
    base_ref[...] = base


def combine_kernel(z_ref, w_ref, base_ref, o_ref):
    main = z_ref.shape[1]
    rows = o_ref.shape[0]
    third = main // 3
    tail_sum = base_ref[:, main:]
    for b in range(3):
        cols = slice(b * third, (b + 1) * third)
        both = mm(w_ref[2 * b * rows : 2 * (b + 1) * rows, :], z_ref[:, cols])
        o_ref[:, cols] = (base_ref[:, cols] + both[:rows]).astype(BF16)
        tail_sum = tail_sum + both[rows:]
    o_ref[:, main:] = tail_sum.astype(BF16)


def bind(kernel, *static):
    def body(*refs):
        kernel(*static, *refs)

    body.__name__ = kernel.__name__
    return body


def params():
    return pltpu.CompilerParams(vmem_limit_bytes=VMEM_LIMIT)


def grid_params():
    return pltpu.CompilerParams(dimension_semantics=("arbitrary",), vmem_limit_bytes=VMEM_LIMIT)


def ring(axis, step):
    count = lax.axis_size(axis)
    return [(i, (i + step) % count) for i in range(count)]


def turn_exchange(blocks, axis, against=False):
    count = len(blocks)
    out = [blocks[0]]
    for d in range(1, count):
        block = blocks[d]
        if against and 2 * d == count:
            for _ in range(d):
                block = lax.ppermute(block, axis, ring(axis, -1))
        else:
            block = lax.ppermute(block, axis, ring(axis, d))
        out.append(block)
    return out


def from_near(x, axis):
    return lax.ppermute(x, axis, ring(axis, 1)), lax.ppermute(x, axis, ring(axis, -1))


def from_far(pairs, axis):
    low = [before[: before.shape[0] // 2] for before, _ in pairs]
    high = [after[after.shape[0] // 2 :] for _, after in pairs]
    if len(pairs) == 1:
        low, high = low[0], high[0]
    else:
        low, high = jnp.concatenate(low, axis=0), jnp.concatenate(high, axis=0)
    return lax.ppermute(low, axis, ring(axis, 1)), lax.ppermute(high, axis, ring(axis, -1))


def exchange(x, axis):
    return lax.all_to_all(x, axis, split_axis=0, concat_axis=0, tiled=True)


def on_device(
    query_vectors,
    attend_lookup_vectors,
    attend_content_vectors,
    forget_speed_dependent,
    amend_speed_dependent,
    result_switch_preactivation,
    feature_forget_baseline,
    amend_speed_baseline,
    sudden_forget_extra,
    group_scaling_factor,
    result_mapping_matrix,
    specialist_tokens_activations,
    specialist_scaling_factor,
    selected_specialists,
    selection_mixing_factors,
    dispatched_switch_matrix,
    dispatched_raising_matrix,
    dispatched_lowering_matrix,
    common_switch_matrix,
    common_raising_matrix,
    common_lowering_matrix,
):
    tok_rows, top_count = selected_specialists.shape
    model = specialist_tokens_activations.shape[1]
    experts = lax.axis_size("ep")
    tp_size = lax.axis_size("tp")
    cap = 3 * tok_rows * top_count // (2 * experts)
    slot_rows = cap * 4 // 3
    main = model * 3 // 4
    third = model // 4
    total = experts * slot_rows

    ff = dispatched_switch_matrix.shape[2]
    me = lax.axis_index("tp").astype(jnp.int32).reshape(1)
    place = lax.axis_index("ep").astype(jnp.int32).reshape(1)

    gate_own, up_own, down_own = (
        dispatched_switch_matrix[0],
        dispatched_raising_matrix[0],
        dispatched_lowering_matrix[0],
    )
    gate_near = from_near(gate_own, "tp")
    up_near = from_near(up_own, "tp")
    down_near = from_near(down_own, "tp")
    both_far = from_far((gate_near, up_near), "tp")
    down_far = from_far((down_near,), "tp")

    normed, outgoing, positions = pl.pallas_call(
        bind(dispatch_kernel, slot_rows, cap),
        out_shape=[
            jax.ShapeDtypeStruct((tok_rows, model), BF16),
            jax.ShapeDtypeStruct((total, main), BF16),
            jax.ShapeDtypeStruct((tok_rows, top_count), jnp.int32),
        ],
        compiler_params=params(),
        name="dispatch",
    )(specialist_tokens_activations, specialist_scaling_factor.reshape(1, -1), selected_specialists.T)

    normed_all = turn_exchange([normed] * tp_size, "tp")

    received = exchange(outgoing.reshape(experts, slot_rows, main), "ep").reshape(total, main)

    out_local, q2, own_state = run_mixer_local(
        query_vectors,
        attend_lookup_vectors,
        attend_content_vectors,
        forget_speed_dependent,
        amend_speed_dependent,
        sudden_forget_extra,
        feature_forget_baseline,
        amend_speed_baseline,
    )
    all_states = lax.all_gather(own_state, "ep")
    starts = run_chain(place, all_states)

    anywhere = pl.BlockSpec(memory_space=pl.ANY)
    in_vmem = pl.BlockSpec(memory_space=pltpu.MemorySpace.VMEM)
    near = tp_size - 1
    kept = experts * cap
    hidden, rows = pl.pallas_call(
        bind(near_kernel, slot_rows, cap),
        in_specs=[in_vmem] + [anywhere] * (2 * near),
        out_shape=[
            jax.ShapeDtypeStruct((kept, near * ff), BF16),
            jax.ShapeDtypeStruct((kept, model), BF16),
        ],
        scratch_shapes=[
            pltpu.VMEM((near, model, ff), BF16),
            pltpu.VMEM((near, model, ff), BF16),
            pltpu.SemaphoreType.DMA((2 * near,)),
        ],
        compiler_params=params(),
        name="near",
    )(received, gate_own, *gate_near, up_own, *up_near)
    downs = (down_own, *down_near, *down_far)
    returning = pl.pallas_call(
        bind(far_kernel, slot_rows, cap),
        in_specs=[anywhere] * (4 + len(downs)),
        out_shape=jax.ShapeDtypeStruct((total, main), BF16),
        scratch_shapes=[
            pltpu.VMEM((kept, model), BF16),
            pltpu.VMEM((kept, tp_size * ff), BF16),
            pltpu.VMEM((model, ff), BF16),
            pltpu.VMEM((model, ff), BF16),
            pltpu.VMEM((tp_size * ff, model), BF16),
            pltpu.VMEM((kept, third), BF16),
            pltpu.SemaphoreType.DMA((6 + len(downs),)),
        ],
        compiler_params=params(),
        name="far",
    )(rows, hidden, *both_far, *downs)
    expert_out = exchange(returning.reshape(experts, slot_rows, main), "ep").reshape(total, main)

    shared_part = pl.pallas_call(
        shared_kernel,
        out_shape=[jax.ShapeDtypeStruct((tok_rows, model), BF16)] * tp_size,
        compiler_params=params(),
        name="shared",
    )(
        *(normed_all[(tp_size - d) % tp_size] for d in range(tp_size)),
        common_switch_matrix,
        common_raising_matrix,
        common_lowering_matrix,
    )
    shared_blocks = turn_exchange(shared_part, "tp")

    mixed_part = run_mixer_final(
        me,
        out_local,
        q2,
        starts,
        result_switch_preactivation,
        group_scaling_factor,
        result_mapping_matrix,
        tp_size,
    )
    mixed_blocks = turn_exchange(mixed_part, "tp", against=True)
    mixed_sum = mixed_blocks[0].astype(F32)
    for block in mixed_blocks[1:]:
        mixed_sum = mixed_sum + block.astype(F32)
    attend_result_matrix = mixed_sum.astype(BF16)
    weights, base = pl.pallas_call(
        bind(prepare_kernel, slot_rows, cap),
        out_shape=[
            jax.ShapeDtypeStruct((6 * tok_rows, total), BF16),
            jax.ShapeDtypeStruct((tok_rows, model), F32),
        ],
        compiler_params=params(),
        name="prepare",
    )(positions, selection_mixing_factors, *shared_blocks)
    moe_out = pl.pallas_call(
        combine_kernel,
        in_specs=[in_vmem] * 3,
        out_shape=jax.ShapeDtypeStruct((tok_rows, model), BF16),
        compiler_params=params(),
        name="combine",
    )(expert_out, weights, base)
    return (attend_result_matrix, moe_out)


def solution(mesh):
    by_rows = P(("grp", "ep"), "tp")
    by_device = P(("grp", "ep", "tp"), None)
    placed = (
        by_rows,
        by_rows,
        by_rows,
        by_rows,
        by_rows,
        by_rows,
        P("tp"),
        P("tp"),
        by_rows,
        P("tp"),
        P("tp", None),
        by_device,
        P(),
        by_device,
        by_device,
        P("ep", None, "tp"),
        P("ep", None, "tp"),
        P("ep", "tp", None),
        P(None, "tp"),
        P(None, "tp"),
        P("tp", None),
    )
    return jax.shard_map(
        on_device, mesh=mesh, in_specs=placed, out_specs=(by_device, by_device), check_vma=False
    )
```

profile of v0, /device:TPU:33, one launch (start us, length us, event | category | flops | bytes accessed | tf_op | source)
XLA Modules:
  0.0 310.0 jit_solution(5585374371908271645)
XLA Ops:
  7.2 3.8 %dispatch.1 = (bf16[128,2048]{1,0:T(8,128)(2,1)}, bf16[512,1536]{1,0:T(8,128)(2,1)}, s32[128,2]{1,0:T(8,128)}) custom-call(bf16[128,2048]{1,0:T(8,128)(2,1)} %refs_0_.1, f32[1,2048]{1,0:T(1,128)} %bitcast.22, s32[2,128]{1,0:T(2,128)} %bitcast.23), custom_call_target="tpu_custom_call" | custom-call | tf_op jit(solution)/shard_map/dispatch/pallas_call | solution.py:567
  11.0 25.5 %all-to-all-start = ((bf16[32,16,1536]{2,1,0:T(8,128)(2,1)}), bf16[32,16,1536]{2,1,0:T(8,128)(2,1)S(1)}, u32[]{:S(2)}, u32[]{:S(2)}) async-start(bf16[32,16,1536]{2,1,0:T(8,128)(2,1)} %bitcast.18), calls=%async_computation | async-start | bytes 3145728 | tf_op jit(solution)/shard_map/all_to_all | solution.py:516
  36.5 0.8 copy.23.x_ref
  37.4 26.4 %mixer_local.1 = (f32[512,512]{1,0:T(8,128)}, bf16[512,512]{1,0:T(8,128)(2,1)}, bf16[512,128]{1,0:T(8,128)(2,1)}) custom-call(bf16[512,512]{1,0:T(8,128)(2,1)} %q_ref.1, bf16[512,512]{1,0:T(8,128)(2,1)} %k_ref.1, bf16[512,512]{1,0:T(8,128)(2,1)} %v_ref.1, bf16[512,512]{1,0:T(8,128)(2,1)} %f_ref.1, bf16[512,512]{1,0:T(8,128)(2,1)} %a_ref.1, ...), custom_call_target="tpu_custom_call" | custom-call | flops 40000000000 | bytes 5000000 | tf_op jit(solution)/shard_map/mixer_local/pallas_call | solution.py:160
  63.9 1.5 collective-permute-start.6
  65.3 1.3 collective-permute-start.4
  66.7 1.3 collective-permute-start.7
  68.0 0.5 collective-permute-start.5
  68.5 1.0 collective-permute-start.10
  69.5 20.5 %collective-permute-done.6.refs_5_ = bf16[2048,256]{1,0:T(8,128)(2,1)S(1)} collective-permute-done((bf16[2048,256]{1,0:T(8,128)(2,1)}, bf16[2048,256]{1,0:T(8,128)(2,1)S(1)}, u32[]{:S(2)}, u32[]{:S(2)}) %collective-permute-start.6) | collective-permute-done | bytes 1048608 | tf_op jit(solution)/shard_map/ppermute | solution.py:502
  90.0 1.2 collective-permute-start.11
  91.3 21.2 %collective-permute-done.4.refs_2_ = bf16[2048,256]{1,0:T(8,128)(2,1)S(1)} collective-permute-done((bf16[2048,256]{1,0:T(8,128)(2,1)}, bf16[2048,256]{1,0:T(8,128)(2,1)S(1)}, u32[]{:S(2)}, u32[]{:S(2)}) %collective-permute-start.4) | collective-permute-done | bytes 1048608 | tf_op jit(solution)/shard_map/ppermute | solution.py:502
  112.5 1.0 copy-done.5
  113.5 1.0 pad_maximum_fusion
  114.7 1.2 pad_maximum_fusion.1
  115.9 2.7 collective-permute-start.9
  118.6 16.3 %collective-permute-done.10.refs_5_ = bf16[256,2048]{1,0:T(8,128)(2,1)S(1)} collective-permute-done((bf16[256,2048]{1,0:T(8,128)(2,1)}, bf16[256,2048]{1,0:T(8,128)(2,1)S(1)}, u32[]{:S(2)}, u32[]{:S(2)}) %collective-permute-start.10) | collective-permute-done | bytes 1048608 | tf_op jit(solution)/shard_map/ppermute | solution.py:502
  134.8 0.9 slice.28
  135.7 0.9 slice.29
  136.9 2.7 collective-permute-start.13
  139.5 1.2 copy-done.1
  140.7 6.9 %near.1 = (bf16[384,768]{1,0:T(8,128)(2,1)}, bf16[384,2048]{1,0:T(8,128)(2,1)}) custom-call(bf16[512,1536]{1,0:T(8,128)(2,1)} %bitcast.17, bf16[2048,256]{1,0:T(8,128)(2,1)} %bitcast.10.refs_1_, bf16[2048,256]{1,0:T(8,128)(2,1)} %copy-done.5, bf16[2048,256]{1,0:T(8,128)(2,1)} %copy-done.7, bf16[2048,256]{1,0:T(8,128)(2,1)} %bitcast.11.refs_4_, ...), custom_call_target="tpu_custom_call" | custom-call | tf_op jit(solution)/shard_map/near/pallas_call | solution.py:599
  147.7 20.9 %collective-permute-done.12.refs_7_ = bf16[128,2048]{1,0:T(8,128)(2,1)S(1)} collective-permute-done((bf16[128,2048]{1,0:T(8,128)(2,1)}, bf16[128,2048]{1,0:T(8,128)(2,1)S(1)}, u32[]{:S(2)}, u32[]{:S(2)}) %collective-permute-start.12) | collective-permute-done | bytes 524320 | tf_op jit(solution)/shard_map/ppermute | solution.py:512
  168.5 0.6 collective-permute-done.13.refs_8_
  169.3 7.6 %far.1 = bf16[512,1536]{1,0:T(8,128)(2,1)} custom-call(bf16[384,2048]{1,0:T(8,128)(2,1)} %get-tuple-element.28.refs_0_, bf16[384,768]{1,0:T(8,128)(2,1)} %get-tuple-element.29.refs_1_, bf16[2048,256]{1,0:T(8,128)(2,1)} %collective-permute-done.8.refs_2_, bf16[2048,256]{1,0:T(8,128)(2,1)} %collective-permute-done.9.refs_3_, bf16[256,2048]{1,0:T(8,128)(2,1)} %bitcast.21, ...), custom_call_target="tpu_custom_call" | custom-call | tf_op jit(solution)/shard_map/far/pallas_call | solution.py:615
  176.9 14.1 %all-to-all-start.1 = ((bf16[32,16,1536]{2,1,0:T(8,128)(2,1)}), bf16[32,16,1536]{2,1,0:T(8,128)(2,1)S(1)}, u32[]{:S(2)}, u32[]{:S(2)}) async-start(bf16[32,16,1536]{2,1,0:T(8,128)(2,1)} %bitcast.15), calls=%async_computation.1 | async-start | bytes 3145728 | tf_op jit(solution)/shard_map/all_to_all | solution.py:516
  191.0 2.7 collective-permute-start.14
  193.7 0.3 collective-permute-start.15
  194.0 0.4 collective-permute-start.16
  194.4 10.7 %collective-permute-done.14.refs_1_ = bf16[128,2048]{1,0:T(8,128)(2,1)S(1)} collective-permute-done((bf16[128,2048]{1,0:T(8,128)(2,1)S(1)}, bf16[128,2048]{1,0:T(8,128)(2,1)S(1)}, u32[]{:S(2)}, u32[]{:S(2)}) %collective-permute-start.14) | collective-permute-done | bytes 524320 | tf_op jit(solution)/shard_map/ppermute | solution.py:496
  205.1 2.6 collective-permute-done.15.refs_2_
  207.7 12.6 %collective-permute-done.16.refs_3_ = bf16[128,2048]{1,0:T(8,128)(2,1)} collective-permute-done((bf16[128,2048]{1,0:T(8,128)(2,1)S(1)}, bf16[128,2048]{1,0:T(8,128)(2,1)}, u32[]{:S(2)}, u32[]{:S(2)}) %collective-permute-start.16) | collective-permute-done | bytes 524320 | tf_op jit(solution)/shard_map/ppermute | solution.py:496
  220.4 4.7 %shared.1 = (bf16[128,2048]{1,0:T(8,128)(2,1)}, bf16[128,2048]{1,0:T(8,128)(2,1)}, bf16[128,2048]{1,0:T(8,128)(2,1)}, bf16[128,2048]{1,0:T(8,128)(2,1)}) custom-call(bf16[128,2048]{1,0:T(8,128)(2,1)} %get-tuple-element.31.refs_0_, bf16[128,2048]{1,0:T(8,128)(2,1)} %copy-done.12, bf16[128,2048]{1,0:T(8,128)(2,1)} %copy-done.13, ...), custom_call_target="tpu_custom_call" | custom-call | tf_op jit(solution)/shard_map/shared/pallas_call | solution.py:633
  225.1 3.4 %chain.1.s_ref = bf16[256,128]{1,0:T(8,128)(2,1)} custom-call(s32[1]{0:T(128)} %bitcast.3.me_ref, bf16[32,512,128]{2,1,0:T(8,128)(2,1)} %bitcast.24), custom_call_target="tpu_custom_call" | custom-call | flops 3000000000 | bytes 4000000 | tf_op jit(solution)/shard_map/chain/pallas_call | solution.py:207
  228.5 8.8 %mixer_final.1 = (bf16[128,2048]{1,0:T(8,128)(2,1)}, bf16[128,2048]{1,0:T(8,128)(2,1)}, bf16[128,2048]{1,0:T(8,128)(2,1)}, bf16[128,2048]{1,0:T(8,128)(2,1)}) custom-call(s32[1]{0:T(128)} %bitcast.me_ref, f32[512,512]{1,0:T(8,128)} %get-tuple-element.20.o_ref, bf16[512,512]{1,0:T(8,128)(2,1)} %get-tuple-element.21.q2_ref, bf16[256,128]{1,0:T(8,128)(2,1)} %chain.1.s_ref, ...), custom_call_target="tpu_custom_call" | custom-call | flops 6000000000 | bytes 8000000 | tf_op jit(solution)/shard_map/mixer_final/pallas_call | solution.py:266
  237.3 2.6 collective-permute-start.1
  240.0 1.2 collective-permute-start.19
  241.2 2.0 collective-permute-start.3
  243.2 19.2 %collective-permute-done.1 = bf16[128,2048]{1,0:T(8,128)(2,1)} collective-permute-done((bf16[128,2048]{1,0:T(8,128)(2,1)}, bf16[128,2048]{1,0:T(8,128)(2,1)}, u32[]{:S(2)}, u32[]{:S(2)}) %collective-permute-start.1) | collective-permute-done | bytes 524320 | tf_op jit(solution)/shard_map/ppermute | solution.py:494
  262.5 3.6 %collective-permute-start.2 = (bf16[128,2048]{1,0:T(8,128)(2,1)}, bf16[128,2048]{1,0:T(8,128)(2,1)}, u32[]{:S(2)}, u32[]{:S(2)}) collective-permute-start(bf16[128,2048]{1,0:T(8,128)(2,1)} %collective-permute-done.1), channel_id=1, source_target_pairs={{0,3},{1,0},{2,1},{3,2},{4,7},{5,4},{6,5},{7,6},{8,11},{9,8},{10,9... | collective-permute-start | bytes 1572872 | tf_op jit(solution)/shard_map/ppermute | solution.py:494
  266.0 0.7 copy.24.refs_1_
  266.8 7.1 %collective-permute-done.19.refs_5_ = bf16[128,2048]{1,0:T(8,128)(2,1)} collective-permute-done((bf16[128,2048]{1,0:T(8,128)(2,1)}, bf16[128,2048]{1,0:T(8,128)(2,1)}, u32[]{:S(2)}, u32[]{:S(2)}) %collective-permute-start.19) | collective-permute-done | bytes 524320 | tf_op jit(solution)/shard_map/ppermute | solution.py:496
  273.8 3.4 %prepare.1 = (bf16[768,512]{1,0:T(8,128)(2,1)}, f32[128,2048]{1,0:T(8,128)}) custom-call(s32[128,2]{1,0:T(8,128)} %get-tuple-element.30.refs_0_, f32[128,2]{1,0:T(8,128)} %copy.24.refs_1_, bf16[128,2048]{1,0:T(8,128)(2,1)} %get-tuple-element.32.refs_2_, bf16[128,2048]{1,0:T(8,128)(2,1)} %copy-done.10, bf16[128,2048]{1,0:T(8,128)(2,1)} %collective-permute-done.18.refs_4_, ...), custom_call_target="tpu_custom_call" | custom-call | tf_op jit(solution)/shard_map/prepare/pallas_call | solution.py:661
  277.2 7.9 %collective-permute-done.3 = bf16[128,2048]{1,0:T(8,128)(2,1)S(1)} collective-permute-done((bf16[128,2048]{1,0:T(8,128)(2,1)}, bf16[128,2048]{1,0:T(8,128)(2,1)S(1)}, u32[]{:S(2)}, u32[]{:S(2)}) %collective-permute-start.3) | collective-permute-done | bytes 524320 | tf_op jit(solution)/shard_map/ppermute | solution.py:496
  285.1 11.2 %collective-permute-done.2 = bf16[128,2048]{1,0:T(8,128)(2,1)} collective-permute-done((bf16[128,2048]{1,0:T(8,128)(2,1)}, bf16[128,2048]{1,0:T(8,128)(2,1)}, u32[]{:S(2)}, u32[]{:S(2)}) %collective-permute-start.2) | collective-permute-done | bytes 524320 | tf_op jit(solution)/shard_map/ppermute | solution.py:494
  296.3 2.3 add_convert_fusion
  298.6 1.2 copy-done
  299.8 3.3 %combine.1 = bf16[128,2048]{1,0:T(8,128)(2,1)} custom-call(bf16[512,1536]{1,0:T(8,128)(2,1)} %bitcast.16, bf16[768,512]{1,0:T(8,128)(2,1)} %get-tuple-element.36.w_ref, f32[128,2048]{1,0:T(8,128)} %get-tuple-element.37.base_ref), custom_call_target="tpu_custom_call" | custom-call | tf_op jit(solution)/shard_map/combine/pallas_call | solution.py:670
  (51 shorter events, 0.8 us)
Async XLA Ops:
  7.2 29.4 %copy-start.14 = (f32[512,8]{0,1:T(8,128)S(1)}, f32[512,8]{0,1:T(8,128)}, u32[]{:S(2)}) copy-start(f32[512,8]{0,1:T(8,128)} %param.29) | copy-start | bytes 49156
  11.0 128.6 %all-to-all-start = ((bf16[32,16,1536]{2,1,0:T(8,128)(2,1)}), bf16[32,16,1536]{2,1,0:T(8,128)(2,1)S(1)}, u32[]{:S(2)}, u32[]{:S(2)}) async-start(bf16[32,16,1536]{2,1,0:T(8,128)(2,1)} %bitcast.18), calls=%async_computation | async-start | bytes 3145728 | tf_op jit(solution)/shard_map/all_to_all | solution.py:516
  36.5 188.6 %all-gather.3.cloned.1.call-start = ((), (), s32[]{:S(2)}) async-start(), calls=%async_computation.2 | async-start | bytes 4325376 | tf_op jit(solution)/shard_map/all_gather | solution.py:592
  63.9 26.1 %collective-permute-start.6 = (bf16[2048,256]{1,0:T(8,128)(2,1)}, bf16[2048,256]{1,0:T(8,128)(2,1)S(1)}, u32[]{:S(2)}, u32[]{:S(2)}) collective-permute-start(bf16[2048,256]{1,0:T(8,128)(2,1)} %bitcast.11.refs_4_), channel_id=1, source_target_pairs={{0,1},{1,2},{2,3},{3,0},{4,5},{5,6},{6,7},{7,4},{8,9},{9,10},{10,1... | collective-permute-start | bytes 3145736 | tf_op jit(solution)/shard_map/ppermute | solution.py:502
  65.3 47.1 %collective-permute-start.4 = (bf16[2048,256]{1,0:T(8,128)(2,1)}, bf16[2048,256]{1,0:T(8,128)(2,1)S(1)}, u32[]{:S(2)}, u32[]{:S(2)}) collective-permute-start(bf16[2048,256]{1,0:T(8,128)(2,1)} %bitcast.10.refs_1_), channel_id=1, source_target_pairs={{0,1},{1,2},{2,3},{3,0},{4,5},{5,6},{6,7},{7,4},{8,9},{9,10},{10,1... | collective-permute-start | bytes 3145736 | tf_op jit(solution)/shard_map/ppermute | solution.py:502
  66.7 47.9 %collective-permute-start.7 = (bf16[2048,256]{1,0:T(8,128)(2,1)}, bf16[2048,256]{1,0:T(8,128)(2,1)S(1)}, u32[]{:S(2)}, u32[]{:S(2)}) collective-permute-start(bf16[2048,256]{1,0:T(8,128)(2,1)} %bitcast.11.refs_4_), channel_id=1, source_target_pairs={{0,3},{1,0},{2,1},{3,2},{4,7},{5,4},{6,5},{7,6},{8,11},{9,8},{10,9... | collective-permute-start | bytes 3145736 | tf_op jit(solution)/shard_map/ppermute | solution.py:502
  68.0 46.6 %collective-permute-start.5 = (bf16[2048,256]{1,0:T(8,128)(2,1)}, bf16[2048,256]{1,0:T(8,128)(2,1)S(1)}, u32[]{:S(2)}, u32[]{:S(2)}) collective-permute-start(bf16[2048,256]{1,0:T(8,128)(2,1)} %bitcast.10.refs_1_), channel_id=1, source_target_pairs={{0,3},{1,0},{2,1},{3,2},{4,7},{5,4},{6,5},{7,6},{8,11},{9,8},{10,9... | collective-permute-start | bytes 3145736 | tf_op jit(solution)/shard_map/ppermute | solution.py:502
  68.5 66.3 %collective-permute-start.10 = (bf16[256,2048]{1,0:T(8,128)(2,1)}, bf16[256,2048]{1,0:T(8,128)(2,1)S(1)}, u32[]{:S(2)}, u32[]{:S(2)}) collective-permute-start(bf16[256,2048]{1,0:T(8,128)(2,1)} %bitcast.19), channel_id=1, source_target_pairs={{0,1},{1,2},{2,3},{3,0},{4,5},{5,6},{6,7},{7,4},{8,9},{9,10},{10,1... | collective-permute-start | bytes 3145736 | tf_op jit(solution)/shard_map/ppermute | solution.py:502
  90.0 1.2 copy-start.3
  90.0 45.7 %collective-permute-start.11 = (bf16[256,2048]{1,0:T(8,128)(2,1)}, bf16[256,2048]{1,0:T(8,128)(2,1)S(1)}, u32[]{:S(2)}, u32[]{:S(2)}) collective-permute-start(bf16[256,2048]{1,0:T(8,128)(2,1)} %bitcast.20), channel_id=1, source_target_pairs={{0,3},{1,0},{2,1},{3,2},{4,7},{5,4},{6,5},{7,6},{8,11},{9,8},{10,9... | collective-permute-start | bytes 3145736 | tf_op jit(solution)/shard_map/ppermute | solution.py:502
  112.5 1.0 copy-start.5
  114.5 54.6 %collective-permute-start.8 = (bf16[2048,256]{1,0:T(8,128)(2,1)}, bf16[2048,256]{1,0:T(8,128)(2,1)}, u32[]{:S(2)}, u32[]{:S(2)}) collective-permute-start(bf16[2048,256]{1,0:T(8,128)(2,1)} %pad_maximum_fusion), channel_id=1, source_target_pairs={{0,1},{1,2},{2,3},{3,0},{4,5},{5,6},{6,7},{7,4},{8,9},{9,10},{10,1... | collective-permute-start | bytes 3145736 | tf_op jit(solution)/shard_map/ppermute | solution.py:512
  114.6 1.4 copy-start.6
  114.6 21.1 %copy-start.7 = (bf16[2048,256]{1,0:T(8,128)(2,1)}, bf16[2048,256]{1,0:T(8,128)(2,1)S(1)}, u32[]{:S(2)}) copy-start(bf16[2048,256]{1,0:T(8,128)(2,1)S(1)} %collective-permute-done.5.refs_3_) | copy-start | bytes 3145732
  115.9 53.2 %collective-permute-start.9 = (bf16[2048,256]{1,0:T(8,128)(2,1)}, bf16[2048,256]{1,0:T(8,128)(2,1)}, u32[]{:S(2)}, u32[]{:S(2)}) collective-permute-start(bf16[2048,256]{1,0:T(8,128)(2,1)} %pad_maximum_fusion.1), channel_id=1, source_target_pairs={{0,3},{1,0},{2,1},{3,2},{4,7},{5,4},{6,5},{7,6},{8,11},{9,8},{10,9... | collective-permute-start | bytes 3145736 | tf_op jit(solution)/shard_map/ppermute | solution.py:512
  134.8 12.8 %copy-start.2 = (bf16[256,2048]{1,0:T(8,128)(2,1)}, bf16[256,2048]{1,0:T(8,128)(2,1)S(1)}, u32[]{:S(2)}) copy-start(bf16[256,2048]{1,0:T(8,128)(2,1)S(1)} %collective-permute-done.10.refs_5_) | copy-start | bytes 3145732
  135.7 32.8 %collective-permute-start.12 = (bf16[128,2048]{1,0:T(8,128)(2,1)}, bf16[128,2048]{1,0:T(8,128)(2,1)S(1)}, u32[]{:S(2)}, u32[]{:S(2)}) collective-permute-start(bf16[128,2048]{1,0:T(8,128)(2,1)} %slice.28), channel_id=1, source_target_pairs={{0,1},{1,2},{2,3},{3,0},{4,5},{5,6},{6,7},{7,4},{8,9},{9,10},{10,1... | collective-permute-start | bytes 1572872 | tf_op jit(solution)/shard_map/ppermute | solution.py:512
  135.7 1.1 copy-start.4
  136.9 32.2 %collective-permute-start.13 = (bf16[128,2048]{1,0:T(8,128)(2,1)}, bf16[128,2048]{1,0:T(8,128)(2,1)}, u32[]{:S(2)}, u32[]{:S(2)}) collective-permute-start(bf16[128,2048]{1,0:T(8,128)(2,1)} %slice.29), channel_id=1, source_target_pairs={{0,3},{1,0},{2,1},{3,2},{4,7},{5,4},{6,5},{7,6},{8,11},{9,8},{10,9... | collective-permute-start | bytes 1572872 | tf_op jit(solution)/shard_map/ppermute | solution.py:512
  139.5 1.2 copy-start.1
  168.5 0.8 copy-start.11
  176.9 14.1 %copy-start.8 = (bf16[128,2048]{1,0:T(8,128)(2,1)S(1)}, bf16[128,2048]{1,0:T(8,128)(2,1)}, u32[]{:S(2)}) copy-start(bf16[128,2048]{1,0:T(8,128)(2,1)} %get-tuple-element.31.refs_0_) | copy-start | bytes 1572868
  176.9 121.7 %all-to-all-start.1 = ((bf16[32,16,1536]{2,1,0:T(8,128)(2,1)}), bf16[32,16,1536]{2,1,0:T(8,128)(2,1)S(1)}, u32[]{:S(2)}, u32[]{:S(2)}) async-start(bf16[32,16,1536]{2,1,0:T(8,128)(2,1)} %bitcast.15), calls=%async_computation.1 | async-start | bytes 3145728 | tf_op jit(solution)/shard_map/all_to_all | solution.py:516
  191.0 14.1 %collective-permute-start.14 = (bf16[128,2048]{1,0:T(8,128)(2,1)S(1)}, bf16[128,2048]{1,0:T(8,128)(2,1)S(1)}, u32[]{:S(2)}, u32[]{:S(2)}) collective-permute-start(bf16[128,2048]{1,0:T(8,128)(2,1)S(1)} %copy-done.8), channel_id=1, source_target_pairs={{0,3},{1,0},{2,1},{3,2},{4,7},{5,4},{6,5},{7,6},{8,11},{9,8},{10,9... | collective-permute-start | bytes 1572872 | tf_op jit(solution)/shard_map/ppermute | solution.py:496
  193.7 14.0 %collective-permute-start.15 = (bf16[128,2048]{1,0:T(8,128)(2,1)S(1)}, bf16[128,2048]{1,0:T(8,128)(2,1)S(1)}, u32[]{:S(2)}, u32[]{:S(2)}) collective-permute-start(bf16[128,2048]{1,0:T(8,128)(2,1)S(1)} %copy-done.8), channel_id=1, source_target_pairs={{0,2},{1,3},{2,0},{3,1},{4,6},{5,7},{6,4},{7,5},{8,10},{9,11},{10,... | collective-permute-start | bytes 1572872 | tf_op jit(solution)/shard_map/ppermute | solution.py:496
  194.0 26.4 %collective-permute-start.16 = (bf16[128,2048]{1,0:T(8,128)(2,1)S(1)}, bf16[128,2048]{1,0:T(8,128)(2,1)}, u32[]{:S(2)}, u32[]{:S(2)}) collective-permute-start(bf16[128,2048]{1,0:T(8,128)(2,1)S(1)} %copy-done.8), channel_id=1, source_target_pairs={{0,1},{1,2},{2,3},{3,0},{4,5},{5,6},{6,7},{7,4},{8,9},{9,10},{10,1... | collective-permute-start | bytes 1572872 | tf_op jit(solution)/shard_map/ppermute | solution.py:496
  205.1 15.3 %copy-start.12 = (bf16[128,2048]{1,0:T(8,128)(2,1)}, bf16[128,2048]{1,0:T(8,128)(2,1)S(1)}, u32[]{:S(2)}) copy-start(bf16[128,2048]{1,0:T(8,128)(2,1)S(1)} %collective-permute-done.14.refs_1_) | copy-start | bytes 1572868
  207.7 12.6 %copy-start.13 = (bf16[128,2048]{1,0:T(8,128)(2,1)}, bf16[128,2048]{1,0:T(8,128)(2,1)S(1)}, u32[]{:S(2)}) copy-start(bf16[128,2048]{1,0:T(8,128)(2,1)S(1)} %collective-permute-done.15.refs_2_) | copy-start | bytes 1572868
  225.1 18.1 %collective-permute-start.17 = (bf16[128,2048]{1,0:T(8,128)(2,1)}, bf16[128,2048]{1,0:T(8,128)(2,1)S(1)}, u32[]{:S(2)}, u32[]{:S(2)}) collective-permute-start(bf16[128,2048]{1,0:T(8,128)(2,1)} %get-tuple-element.33), channel_id=1, source_target_pairs={{0,1},{1,2},{2,3},{3,0},{4,5},{5,6},{6,7},{7,4},{8,9},{9,10},{10,1... | collective-permute-start | bytes 1572872 | tf_op jit(solution)/shard_map/ppermute | solution.py:496
  228.5 37.5 %copy-start.15 = (f32[128,2]{0,1:T(2,128)S(1)}, f32[128,2]{0,1:T(2,128)}, u32[]{:S(2)}) copy-start(f32[128,2]{0,1:T(2,128)} %param.35) | copy-start | bytes 3076
  237.3 59.0 %copy-start.9 = (bf16[128,2048]{1,0:T(8,128)(2,1)S(1)}, bf16[128,2048]{1,0:T(8,128)(2,1)}, u32[]{:S(2)}) copy-start(bf16[128,2048]{1,0:T(8,128)(2,1)} %get-tuple-element.23) | copy-start | bytes 1572868
  237.3 25.1 %collective-permute-start.1 = (bf16[128,2048]{1,0:T(8,128)(2,1)}, bf16[128,2048]{1,0:T(8,128)(2,1)}, u32[]{:S(2)}, u32[]{:S(2)}) collective-permute-start(bf16[128,2048]{1,0:T(8,128)(2,1)} %get-tuple-element.25), channel_id=1, source_target_pairs={{0,3},{1,0},{2,1},{3,2},{4,7},{5,4},{6,5},{7,6},{8,11},{9,8},{10,9... | collective-permute-start | bytes 1572872 | tf_op jit(solution)/shard_map/ppermute | solution.py:494
  240.0 26.8 %collective-permute-start.18 = (bf16[128,2048]{1,0:T(8,128)(2,1)}, bf16[128,2048]{1,0:T(8,128)(2,1)}, u32[]{:S(2)}, u32[]{:S(2)}) collective-permute-start(bf16[128,2048]{1,0:T(8,128)(2,1)} %get-tuple-element.34), channel_id=1, source_target_pairs={{0,2},{1,3},{2,0},{3,1},{4,6},{5,7},{6,4},{7,5},{8,10},{9,11},{10,... | collective-permute-start | bytes 1572872 | tf_op jit(solution)/shard_map/ppermute | solution.py:496
  240.0 33.9 %collective-permute-start.19 = (bf16[128,2048]{1,0:T(8,128)(2,1)}, bf16[128,2048]{1,0:T(8,128)(2,1)}, u32[]{:S(2)}, u32[]{:S(2)}) collective-permute-start(bf16[128,2048]{1,0:T(8,128)(2,1)} %get-tuple-element.35), channel_id=1, source_target_pairs={{0,3},{1,0},{2,1},{3,2},{4,7},{5,4},{6,5},{7,6},{8,11},{9,8},{10,9... | collective-permute-start | bytes 1572872 | tf_op jit(solution)/shard_map/ppermute | solution.py:496
  241.2 43.9 %collective-permute-start.3 = (bf16[128,2048]{1,0:T(8,128)(2,1)}, bf16[128,2048]{1,0:T(8,128)(2,1)S(1)}, u32[]{:S(2)}, u32[]{:S(2)}) collective-permute-start(bf16[128,2048]{1,0:T(8,128)(2,1)} %get-tuple-element.26), channel_id=1, source_target_pairs={{0,3},{1,0},{2,1},{3,2},{4,7},{5,4},{6,5},{7,6},{8,11},{9,8},{10,9... | collective-permute-start | bytes 1572872 | tf_op jit(solution)/shard_map/ppermute | solution.py:496
  243.2 30.6 %copy-start.10 = (bf16[128,2048]{1,0:T(8,128)(2,1)}, bf16[128,2048]{1,0:T(8,128)(2,1)S(1)}, u32[]{:S(2)}) copy-start(bf16[128,2048]{1,0:T(8,128)(2,1)S(1)} %collective-permute-done.17.refs_3_) | copy-start | bytes 1572868
  243.2 41.9 %collective-permute-start = (bf16[128,2048]{1,0:T(8,128)(2,1)}, bf16[128,2048]{1,0:T(8,128)(2,1)}, u32[]{:S(2)}, u32[]{:S(2)}) collective-permute-start(bf16[128,2048]{1,0:T(8,128)(2,1)} %get-tuple-element.24), channel_id=1, source_target_pairs={{0,1},{1,2},{2,3},{3,0},{4,5},{5,6},{6,7},{7,4},{8,9},{9,10},{10,1... | collective-permute-start | bytes 1572872 | tf_op jit(solution)/shard_map/ppermute | solution.py:496
  262.5 33.8 %collective-permute-start.2 = (bf16[128,2048]{1,0:T(8,128)(2,1)}, bf16[128,2048]{1,0:T(8,128)(2,1)}, u32[]{:S(2)}, u32[]{:S(2)}) collective-permute-start(bf16[128,2048]{1,0:T(8,128)(2,1)} %collective-permute-done.1), channel_id=1, source_target_pairs={{0,3},{1,0},{2,1},{3,2},{4,7},{5,4},{6,5},{7,6},{8,11},{9,8},{10,9... | collective-permute-start | bytes 1572872 | tf_op jit(solution)/shard_map/ppermute | solution.py:494
  298.6 1.2 copy-start
Sparse Core Ops, SparseCore 0:
  64.0 89.4 all-gather.2
where the time goes:
time: 311 us; the launch traced here: 310 us
  waiting for transfers between devices  151 us (49%)
  Pallas kernels  68.3 us (22%)
  starting transfers between devices  64.6 us (21%)
  between operations  14.2 us (5%)
  local copies, waits for them, and re-layouts  7.4 us (2%)
  other arithmetic  4.56 us (1%)
    ppermute x3, waiting for transfers between devices, from_near(): lax.ppermute(x, axis, ring(axis, 1))  58 us
    ppermute x8, waiting for transfers between devices, turn_exchange(): block = lax.ppermute(block, axis, ring(axis, d))  40.9 us
    all_to_all x2, starting transfers between devices, exchange(): return lax.all_to_all(x, axis, split_axis=0, concat_axis=0, tiled=True)  39.5 us
    ppermute x2, waiting for transfers between devices, turn_exchange(): block = lax.ppermute(block, axis, ring(axis, -1))  30.5 us
    pallas_call x1, Pallas kernels, run_mixer_local(): pl.pallas_call(mixer_local, grid=(pairs,), in_specs=[spec] * 5 + [pl.Bloc...  26.4 us
    ppermute x2, waiting for transfers between devices, from_far(): lax.ppermute(low, axis, ring(axis, 1))  20.9 us
    pallas_call x1, Pallas kernels, run_mixer_final(): pl.pallas_call(mixer_final, grid_spec=pltpu.PrefetchScalarGridSpec(num_sc...  8.78 us
    pallas_call x1, Pallas kernels, on_device(): pl.pallas_call(bind(far_kernel, slot_rows, cap), in_specs=[anywhere] * (4...  7.57 us
  transfers between devices with their start and end apart: 23, of which 12 were waited for; matrix products, arithmetic and copies ran while one was open for 3% of the time, Pallas kernels for 20%

commit v1 on v0

--- a/solution.py
+++ b/solution.py
@@ -10,6 +10,7 @@
 BF16 = jnp.bfloat16
 SPAN = 64
 VMEM_LIMIT = 56 * 1024 * 1024
+SMALL_LIMIT = 20 * 1024 * 1024
 
 
 def mm(a, b):
@@ -169,7 +170,7 @@
         ],
         scratch_shapes=[pltpu.VMEM((2 * SPAN, wide), F32)],
         compiler_params=pltpu.CompilerParams(
-            dimension_semantics=("arbitrary",), vmem_limit_bytes=VMEM_LIMIT
+            dimension_semantics=("arbitrary",), vmem_limit_bytes=SMALL_LIMIT
         ),
         cost_estimate=pl.CostEstimate(
             flops=40_000_000_000, transcendentals=2_000_000, bytes_accessed=5_000_000
@@ -332,35 +333,14 @@
         out_ref[:, b * third : (b + 1) * third] = mm_tn(hot2, data).astype(BF16)
 
 
-class Copies:
-    def __init__(self, sems):
-        self.sems = sems
-        self.made = []
-
-    def start(self, src, dst, group):
-        copy = pltpu.make_async_copy(src, dst, self.sems.at[len(self.made)])
-        copy.start()
-        self.made.append((group, copy))
-
-    def wait(self, group):
-        for at, copy in self.made:
-            if at == group:
-                copy.wait()
-
-
 def near_kernel(slot_rows, cap, r_ref, *refs):
-    blocks = (len(refs) - 5) // 2
-    gates, ups = refs[:blocks], refs[blocks : 2 * blocks]
-    h_ref, x_ref, g_ref, u_ref, sems = refs[2 * blocks :]
+    *others, h_ref, x_ref = refs
+    count = len(others) // 2
     total, main = r_ref.shape
     third = main // 3
-    ff = g_ref.shape[2]
+    ff = others[0].shape[1]
     size = min(256, total)
     kept = size // slot_rows * cap
-    copies = Copies(sems)
-    for k in range(blocks):
-        copies.start(gates[k], g_ref.at[k], k)
-        copies.start(ups[k], u_ref.at[k], k)
     whole, tails = picks(size, slot_rows, cap)
     for i in range(total // size):
         rows = slice(i * kept, (i + 1) * kept)
@@ -370,43 +350,47 @@
         for b in range(3):
             acc = acc + mm(tails[b], block[:, b * third : (b + 1) * third])
         x_ref[rows, main:] = acc.astype(BF16)
-    for k in range(blocks):
-        copies.wait(k)
-        gate = mm(x_ref[...], g_ref[k])
-        up = mm(x_ref[...], u_ref[k])
+    for k in range(count):
+        gate = mm(x_ref[...], others[k][...])
+        up = mm(x_ref[...], others[count + k][...])
         h_ref[:, k * ff : (k + 1) * ff] = (gate * sigmoid(gate) * up).astype(BF16)
 
 
-def far_kernel(slot_rows, cap, x_hbm, h_hbm, fa, fb, *refs):
-    *downs, o_ref, x_ref, h_ref, g_ref, u_ref, d_ref, tail_ref, sems = refs
+def far_kernel(slot_rows, cap, x_ref, h_ref, gate_ref, up_ref, fa_ref, fb_ref, *refs):
+    *downs, o_ref, f_ref, tail_ref = refs
     total, main = o_ref.shape
     third = main // 3
-    model, ff = g_ref.shape
-    near = h_ref.shape[1] - ff
-    half = model // 2
+    half = fa_ref.shape[0] // 2
+    ff = gate_ref.shape[1]
     size = min(256, total)
     kept = size // slot_rows * cap
-    copies = Copies(sems)
-    copies.start(x_hbm, x_ref, "x")
-    for src, at in ((fa, 0), (fb, half)):
-        copies.start(src.at[0:half, :], g_ref.at[at : at + half, :], "x")
-        copies.start(src.at[half:model, :], u_ref.at[at : at + half, :], "x")
-    copies.start(h_hbm, h_ref.at[:, 0:near], "d")
-    base = 0
-    for src in downs:
-        rows = src.shape[0]
-        copies.start(src, d_ref.at[base : base + rows, :], "d")
-        base += rows
     whole, tails = picks(size, slot_rows, cap)
-    copies.wait("x")
-    gate = mm(x_ref[...], g_ref[...])
-    up = mm(x_ref[...], u_ref[...])
-    copies.wait("d")
-    h_ref[:, near:] = (gate * sigmoid(gate) * up).astype(BF16)
-    tail_ref[...] = mm(h_ref[...], d_ref[:, main:]).astype(BF16)
+    gate = mm(x_ref[...], gate_ref[...])
+    up = mm(x_ref[...], up_ref[...])
+    f_ref[:, :ff] = (gate * sigmoid(gate) * up).astype(BF16)
+    low, high = x_ref[:, :half], x_ref[:, half:]
+    gate = mm(low, fa_ref[:half]) + mm(high, fb_ref[:half])
+    up = mm(low, fa_ref[half:]) + mm(high, fb_ref[half:])
+    f_ref[:, ff:] = (gate * sigmoid(gate) * up).astype(BF16)
+
+    def lower(cols):
+        acc = None
+        at = 0
+        for d_ref in downs:
+            count = d_ref.shape[0]
+            if at < h_ref.shape[1]:
+                h = h_ref[:, at : at + count]
+            else:
+                h = f_ref[:, at - h_ref.shape[1] : at - h_ref.shape[1] + count]
+            part = mm(h, d_ref[:, cols])
+            acc = part if acc is None else acc + part
+            at += count
+        return acc.astype(BF16)
+
+    tail_ref[...] = lower(slice(main, main + third))
     for b in range(3):
         cols = slice(b * third, (b + 1) * third)
-        y = mm(h_ref[...], d_ref[:, cols]).astype(BF16)
+        y = lower(cols)
         spread = jnp.concatenate([whole, tails[b]], axis=0)
         for i in range(total // size):
             rows = slice(i * kept, (i + 1) * kept)
@@ -415,7 +399,7 @@
 
 
 def shared_kernel(*refs):
-    count = (len(refs) - 3) // 2
+    count = len(refs) // 2 - 1
     rows_in, outs = refs[:count], refs[count + 3 :]
     g_ref, u_ref, d_ref = refs[count : count + 3]
     x = jnp.concatenate([ref[...] for ref in rows_in], axis=0)
@@ -471,8 +455,8 @@
     return body
 
 
-def params():
-    return pltpu.CompilerParams(vmem_limit_bytes=VMEM_LIMIT)
+def params(limit=VMEM_LIMIT):
+    return pltpu.CompilerParams(vmem_limit_bytes=limit)
 
 
 def grid_params():
@@ -484,18 +468,8 @@
     return [(i, (i + step) % count) for i in range(count)]
 
 
-def turn_exchange(blocks, axis, against=False):
-    count = len(blocks)
-    out = [blocks[0]]
-    for d in range(1, count):
-        block = blocks[d]
-        if against and 2 * d == count:
-            for _ in range(d):
-                block = lax.ppermute(block, axis, ring(axis, -1))
-        else:
-            block = lax.ppermute(block, axis, ring(axis, d))
-        out.append(block)
-    return out
+def turn_exchange(blocks, axis):
+    return [blocks[0]] + [lax.ppermute(blocks[d], axis, ring(axis, d)) for d in range(1, len(blocks))]
 
 
 def from_near(x, axis):
@@ -575,7 +549,8 @@
         name="dispatch",
     )(specialist_tokens_activations, specialist_scaling_factor.reshape(1, -1), selected_specialists.T)
 
-    normed_all = turn_exchange([normed] * tp_size, "tp")
+    normed_near = from_near(normed, "tp")
+    normed_far = from_far((normed_near,), "tp")
 
     received = exchange(outgoing.reshape(experts, slot_rows, main), "ep").reshape(total, main)
 
@@ -592,42 +567,28 @@
     all_states = lax.all_gather(own_state, "ep")
     starts = run_chain(place, all_states)
 
-    anywhere = pl.BlockSpec(memory_space=pl.ANY)
     in_vmem = pl.BlockSpec(memory_space=pltpu.MemorySpace.VMEM)
-    near = tp_size - 1
     kept = experts * cap
     hidden, rows = pl.pallas_call(
         bind(near_kernel, slot_rows, cap),
-        in_specs=[in_vmem] + [anywhere] * (2 * near),
+        in_specs=[in_vmem] * 5,
+        out_specs=[in_vmem] * 2,
         out_shape=[
-            jax.ShapeDtypeStruct((kept, near * ff), BF16),
+            jax.ShapeDtypeStruct((kept, 2 * ff), BF16),
             jax.ShapeDtypeStruct((kept, model), BF16),
         ],
-        scratch_shapes=[
-            pltpu.VMEM((near, model, ff), BF16),
-            pltpu.VMEM((near, model, ff), BF16),
-            pltpu.SemaphoreType.DMA((2 * near,)),
-        ],
-        compiler_params=params(),
+        compiler_params=params(SMALL_LIMIT),
         name="near",
-    )(received, gate_own, *gate_near, up_own, *up_near)
-    downs = (down_own, *down_near, *down_far)
+    )(received, *gate_near, *up_near)
+    downs = (*down_near, down_own, *down_far)
     returning = pl.pallas_call(
         bind(far_kernel, slot_rows, cap),
-        in_specs=[anywhere] * (4 + len(downs)),
+        in_specs=[in_vmem] * (6 + len(downs)),
         out_shape=jax.ShapeDtypeStruct((total, main), BF16),
-        scratch_shapes=[
-            pltpu.VMEM((kept, model), BF16),
-            pltpu.VMEM((kept, tp_size * ff), BF16),
-            pltpu.VMEM((model, ff), BF16),
-            pltpu.VMEM((model, ff), BF16),
-            pltpu.VMEM((tp_size * ff, model), BF16),
-            pltpu.VMEM((kept, third), BF16),
-            pltpu.SemaphoreType.DMA((6 + len(downs),)),
-        ],
-        compiler_params=params(),
+        scratch_shapes=[pltpu.VMEM((kept, 2 * ff), BF16), pltpu.VMEM((kept, third), BF16)],
+        compiler_params=params(SMALL_LIMIT),
         name="far",
-    )(rows, hidden, *both_far, *downs)
+    )(rows, hidden, gate_own, up_own, *both_far, *downs)
     expert_out = exchange(returning.reshape(experts, slot_rows, main), "ep").reshape(total, main)
 
     shared_part = pl.pallas_call(
@@ -636,7 +597,10 @@
         compiler_params=params(),
         name="shared",
     )(
-        *(normed_all[(tp_size - d) % tp_size] for d in range(tp_size)),
+        normed,
+        normed_near[1],
+        *normed_far,
+        normed_near[0],
         common_switch_matrix,
         common_raising_matrix,
         common_lowering_matrix,
@@ -653,7 +617,7 @@
         result_mapping_matrix,
         tp_size,
     )
-    mixed_blocks = turn_exchange(mixed_part, "tp", against=True)
+    mixed_blocks = turn_exchange(mixed_part, "tp")
     mixed_sum = mixed_blocks[0].astype(F32)
     for block in mixed_blocks[1:]:
         mixed_sum = mixed_sum + block.astype(F32)

time: 311 us -> 287 us (0.923)
  waiting for transfers between devices: 151 us -> 122 us
  local copies, waits for them, and re-layouts: 7.4 us -> 17.3 us
  Pallas kernels: 68.3 us -> 64 us
    ppermute x10 -> x6, waiting for transfers between devices: 71.4 us -> 26.8 us  [turn_exchange(): lax.ppermute(blocks[d], axis, ring(axis, d))]
    ppermute x3 -> x4, waiting for transfers between devices: 58 us -> 68.3 us  [from_near(): lax.ppermute(x, axis, ring(axis, 1))]
    unnamed x34 -> x64, local copies, waits for them, and re-layouts: 5.48 us -> 14.5 us
    ppermute x10 -> x6, starting transfers between devices: 12.8 us -> 6.06 us  [turn_exchange(): lax.ppermute(blocks[d], axis, ring(axis, d))]
    ppermute x2 -> x3, waiting for transfers between devices: 20.9 us -> 26.4 us  [from_far(): lax.ppermute(low, axis, ring(axis, 1))]
    pallas_call x2, Pallas kernels: 14.5 us -> 10.9 us  [the longest x1 8.44 us: on_device(): pl.pallas_call(bind(far_kernel, slot_rows, cap), in_specs=[in_vmem] * (6...]
    ppermute x2 -> x3, starting transfers between devices: 5.34 us -> 8.12 us  [from_far(): lax.ppermute(high, axis, ring(axis, -1))]
  transfers between devices with their start and end apart: 23 -> 23, of which waited for: 12 -> 11; matrix products, arithmetic and copies ran while one was open for 3% -> 3% of each run, Pallas kernels for 20% -> 20%
where the time goes in v1:
time: 287 us; the launch traced here: 286 us
  waiting for transfers between devices  122 us (43%)
  Pallas kernels  64 us (22%)
  starting transfers between devices  63.6 us (22%)
  local copies, waits for them, and re-layouts  17.3 us (6%)
  between operations  14.4 us (5%)
  other arithmetic  4.8 us (2%)
    ppermute x4, waiting for transfers between devices, from_near(): lax.ppermute(x, axis, ring(axis, 1))  68.3 us
    all_to_all x2, starting transfers between devices, exchange(): return lax.all_to_all(x, axis, split_axis=0, concat_axis=0, tiled=True)  39.7 us
    ppermute x6, waiting for transfers between devices, turn_exchange(): lax.ppermute(blocks[d], axis, ring(axis, d))  26.8 us
    ppermute x3, waiting for transfers between devices, from_far(): lax.ppermute(low, axis, ring(axis, 1))  26.4 us
    pallas_call x1, Pallas kernels, run_mixer_local(): pl.pallas_call(mixer_local, grid=(pairs,), in_specs=[spec] * 5 + [pl.Bloc...  25.5 us
    unnamed x64, local copies, waits for them, and re-layouts  14.5 us
    pallas_call x1, Pallas kernels, run_mixer_final(): pl.pallas_call(mixer_final, grid_spec=pltpu.PrefetchScalarGridSpec(num_sc...  8.79 us
    pallas_call x1, Pallas kernels, on_device(): pl.pallas_call(bind(far_kernel, slot_rows, cap), in_specs=[in_vmem] * (6...  8.44 us
  transfers between devices with their start and end apart: 23, of which 11 were waited for; matrix products, arithmetic and copies ran while one was open for 3% of the time, Pallas kernels for 20%

profile of v1, /device:TPU:33, one launch (start us, length us, event | category | flops | bytes accessed | tf_op | source)
XLA Modules:
  0.0 286.2 jit_solution(771845271934645088)
XLA Ops:
  7.2 3.9 %dispatch.1 = (bf16[128,2048]{1,0:T(8,128)(2,1)}, bf16[512,1536]{1,0:T(8,128)(2,1)}, s32[128,2]{1,0:T(8,128)}) custom-call(bf16[128,2048]{1,0:T(8,128)(2,1)} %refs_0_.1, f32[1,2048]{1,0:T(1,128)} %bitcast.23, s32[2,128]{1,0:T(2,128)} %bitcast.24), custom_call_target="tpu_custom_call" | custom-call | tf_op jit(solution)/shard_map/dispatch/pallas_call | solution.py:541
  11.1 25.5 %all-to-all-start = ((bf16[32,16,1536]{2,1,0:T(8,128)(2,1)}), bf16[32,16,1536]{2,1,0:T(8,128)(2,1)S(1)}, u32[]{:S(2)}, u32[]{:S(2)}) async-start(bf16[32,16,1536]{2,1,0:T(8,128)(2,1)} %bitcast.22), calls=%async_computation | async-start | bytes 3145728 | tf_op jit(solution)/shard_map/all_to_all | solution.py:490
  36.9 1.0 copy-done.14
  37.9 1.0 copy-done.15
  39.0 25.5 %mixer_local.1 = (f32[512,512]{1,0:T(8,128)S(1)}, bf16[512,512]{1,0:T(8,128)(2,1)S(1)}, bf16[512,128]{1,0:T(8,128)(2,1)}) custom-call(bf16[512,512]{1,0:T(8,128)(2,1)S(1)} %copy-done.11, bf16[512,512]{1,0:T(8,128)(2,1)S(1)} %copy-done.12, bf16[512,512]{1,0:T(8,128)(2,1)S(1)} %copy-done.13, bf16[512,512]{1,0:T(8,128)(2,1)S(1)} %copy-done.14, ...), custom_call_target="tpu_custom_call" | custom-call | flops 40000000000 | bytes 5000000 | tf_op jit(solution)/shard_map/mixer_local/pallas_call | solution.py:161
  64.5 1.0 copy-done.18
  66.3 1.5 collective-permute-start.5
  67.8 1.3 collective-permute-start.3
  69.1 1.3 collective-permute-start.6
  70.9 1.0 collective-permute-start.9
  71.9 20.5 %collective-permute-done.5.refs_3_ = bf16[2048,256]{1,0:T(8,128)(2,1)S(1)} collective-permute-done((bf16[2048,256]{1,0:T(8,128)(2,1)}, bf16[2048,256]{1,0:T(8,128)(2,1)S(1)}, u32[]{:S(2)}, u32[]{:S(2)}) %collective-permute-start.5) | collective-permute-done | bytes 1048608 | tf_op jit(solution)/shard_map/ppermute | solution.py:476
  92.5 1.2 collective-permute-start.10
  93.7 1.0 copy-done.2
  94.7 20.1 %collective-permute-done.3.refs_1_ = bf16[2048,256]{1,0:T(8,128)(2,1)S(1)} collective-permute-done((bf16[2048,256]{1,0:T(8,128)(2,1)}, bf16[2048,256]{1,0:T(8,128)(2,1)S(1)}, u32[]{:S(2)}, u32[]{:S(2)}) %collective-permute-start.3) | collective-permute-done | bytes 1048608 | tf_op jit(solution)/shard_map/ppermute | solution.py:476
  114.9 1.0 copy-done.4
  115.9 1.1 pad_maximum_fusion
  117.1 1.2 pad_maximum_fusion.1
  118.3 2.7 collective-permute-start.8
  121.0 16.4 %collective-permute-done.9.refs_6_ = bf16[256,2048]{1,0:T(8,128)(2,1)S(1)} collective-permute-done((bf16[256,2048]{1,0:T(8,128)(2,1)}, bf16[256,2048]{1,0:T(8,128)(2,1)S(1)}, u32[]{:S(2)}, u32[]{:S(2)}) %collective-permute-start.9) | collective-permute-done | bytes 1048608 | tf_op jit(solution)/shard_map/ppermute | solution.py:476
  137.4 0.9 slice.36
  138.3 0.9 slice.37
  139.4 2.7 collective-permute-start.12
  142.1 1.2 copy-done.3
  143.4 1.2 copy-done.5
  144.6 1.2 copy-done.7
  145.8 1.2 copy-done.9
  147.0 2.5 near.1
  149.5 21.5 %collective-permute-done.11.refs_9_ = bf16[128,2048]{1,0:T(8,128)(2,1)S(1)} collective-permute-done((bf16[128,2048]{1,0:T(8,128)(2,1)}, bf16[128,2048]{1,0:T(8,128)(2,1)S(1)}, u32[]{:S(2)}, u32[]{:S(2)}) %collective-permute-start.11) | collective-permute-done | bytes 524320 | tf_op jit(solution)/shard_map/ppermute | solution.py:486
  171.6 8.4 %far.1 = bf16[512,1536]{1,0:T(8,128)(2,1)} custom-call(bf16[384,2048]{1,0:T(8,128)(2,1)S(1)} %get-tuple-element.28.refs_0_, bf16[384,512]{1,0:T(8,128)(2,1)S(1)} %get-tuple-element.29.refs_1_, bf16[2048,256]{1,0:T(8,128)(2,1)} %bitcast.10.refs_2_, bf16[2048,256]{1,0:T(8,128)(2,1)} %bitcast.11.refs_3_, bf16[2048,256]{1,0:T(8,128)(2,1)} %collective-permute-done.7.refs_4_, ...), custom_call_target="tpu_custom_call" | custom-call | tf_op jit(solution)/shard_map/far/pallas_call | solution.py:584
  180.0 14.3 %all-to-all-start.1 = ((bf16[32,16,1536]{2,1,0:T(8,128)(2,1)}), bf16[32,16,1536]{2,1,0:T(8,128)(2,1)S(1)}, u32[]{:S(2)}, u32[]{:S(2)}) async-start(bf16[32,16,1536]{2,1,0:T(8,128)(2,1)} %bitcast.13), calls=%async_computation.1 | async-start | bytes 3145728 | tf_op jit(solution)/shard_map/all_to_all | solution.py:490
  194.3 1.2 collective-permute-start.14
  195.5 1.6 collective-permute-start.13
  197.1 11.3 %collective-permute-done.14.refs_4_ = bf16[128,2048]{1,0:T(8,128)(2,1)S(1)} collective-permute-done((bf16[128,2048]{1,0:T(8,128)(2,1)S(1)}, bf16[128,2048]{1,0:T(8,128)(2,1)S(1)}, u32[]{:S(2)}, u32[]{:S(2)}) %collective-permute-start.14) | collective-permute-done | bytes 524320 | tf_op jit(solution)/shard_map/ppermute | solution.py:476
  209.2 2.8 collective-permute-start.16
  212.0 4.9 %collective-permute-done.15.refs_2_ = bf16[64,2048]{1,0:T(8,128)(2,1)S(1)} collective-permute-done((bf16[64,2048]{1,0:T(8,128)(2,1)}, bf16[64,2048]{1,0:T(8,128)(2,1)S(1)}, u32[]{:S(2)}, u32[]{:S(2)}) %collective-permute-start.15) | collective-permute-done | bytes 262176 | tf_op jit(solution)/shard_map/ppermute | solution.py:486
  218.3 4.8 %shared.1 = (bf16[128,2048]{1,0:T(8,128)(2,1)}, bf16[128,2048]{1,0:T(8,128)(2,1)}, bf16[128,2048]{1,0:T(8,128)(2,1)}, bf16[128,2048]{1,0:T(8,128)(2,1)}) custom-call(bf16[128,2048]{1,0:T(8,128)(2,1)} %get-tuple-element.31.refs_0_, bf16[128,2048]{1,0:T(8,128)(2,1)} %copy-done.22, bf16[64,2048]{1,0:T(8,128)(2,1)} %copy-done.27, bf16[64,2048]{1,0:T(8,128)(2,1)} %copy-done.28, ...), custom_call_target="tpu_custom_call" | custom-call | tf_op jit(solution)/shard_map/shared/pallas_call | solution.py:594
  223.1 2.8 collective-permute-start.18
  225.9 3.4 %chain.1.s_ref = bf16[256,128]{1,0:T(8,128)(2,1)} custom-call(s32[1]{0:T(128)} %bitcast.3.me_ref, bf16[32,512,128]{2,1,0:T(8,128)(2,1)} %bitcast.25), custom_call_target="tpu_custom_call" | custom-call | flops 3000000000 | bytes 4000000 | tf_op jit(solution)/shard_map/chain/pallas_call | solution.py:208
  229.3 8.8 %mixer_final.1 = (bf16[128,2048]{1,0:T(8,128)(2,1)}, bf16[128,2048]{1,0:T(8,128)(2,1)}, bf16[128,2048]{1,0:T(8,128)(2,1)}, bf16[128,2048]{1,0:T(8,128)(2,1)}) custom-call(s32[1]{0:T(128)} %bitcast.me_ref, f32[512,512]{1,0:T(8,128)} %copy-done.18, bf16[512,512]{1,0:T(8,128)(2,1)} %copy-done.19, bf16[256,128]{1,0:T(8,128)(2,1)} %chain.1.s_ref, ...), custom_call_target="tpu_custom_call" | custom-call | flops 6000000000 | bytes 8000000 | tf_op jit(solution)/shard_map/mixer_final/pallas_call | solution.py:267
  238.8 2.6 collective-permute-start.1
  242.2 4.5 %collective-permute-done.18.refs_4_ = bf16[128,2048]{1,0:T(8,128)(2,1)S(1)} collective-permute-done((bf16[128,2048]{1,0:T(8,128)(2,1)}, bf16[128,2048]{1,0:T(8,128)(2,1)S(1)}, u32[]{:S(2)}, u32[]{:S(2)}) %collective-permute-start.18) | collective-permute-done | bytes 524320 | tf_op jit(solution)/shard_map/ppermute | solution.py:472
  246.7 2.3 collective-permute-done.19.refs_5_
  249.0 3.4 %prepare.1 = (bf16[768,512]{1,0:T(8,128)(2,1)}, f32[128,2048]{1,0:T(8,128)}) custom-call(s32[128,2]{1,0:T(8,128)} %get-tuple-element.30.refs_0_, f32[128,2]{1,0:T(8,128)} %copy.24.refs_1_, bf16[128,2048]{1,0:T(8,128)(2,1)} %get-tuple-element.32.refs_2_, bf16[128,2048]{1,0:T(8,128)(2,1)} %copy-done.24, bf16[128,2048]{1,0:T(8,128)(2,1)} %copy-done.25, ...), custom_call_target="tpu_custom_call" | custom-call | tf_op jit(solution)/shard_map/prepare/pallas_call | solution.py:625
  252.4 10.0 %collective-permute-done.2 = bf16[128,2048]{1,0:T(8,128)(2,1)} collective-permute-done((bf16[128,2048]{1,0:T(8,128)(2,1)}, bf16[128,2048]{1,0:T(8,128)(2,1)}, u32[]{:S(2)}, u32[]{:S(2)}) %collective-permute-start.2) | collective-permute-done | bytes 524320 | tf_op jit(solution)/shard_map/ppermute | solution.py:472
  262.3 10.0 %collective-permute-done = bf16[128,2048]{1,0:T(8,128)(2,1)} collective-permute-done((bf16[128,2048]{1,0:T(8,128)(2,1)}, bf16[128,2048]{1,0:T(8,128)(2,1)}, u32[]{:S(2)}, u32[]{:S(2)}) %collective-permute-start) | collective-permute-done | bytes 524320 | tf_op jit(solution)/shard_map/ppermute | solution.py:472
  272.3 2.5 add_convert_fusion
  274.8 1.2 copy-done.20
  276.0 3.3 %combine.1 = bf16[128,2048]{1,0:T(8,128)(2,1)} custom-call(bf16[512,1536]{1,0:T(8,128)(2,1)} %bitcast.21, bf16[768,512]{1,0:T(8,128)(2,1)} %get-tuple-element.36.w_ref, f32[128,2048]{1,0:T(8,128)} %get-tuple-element.37.base_ref), custom_call_target="tpu_custom_call" | custom-call | tf_op jit(solution)/shard_map/combine/pallas_call | solution.py:634
  (83 shorter events, 6.2 us)
Async XLA Ops:
  7.2 29.5 %copy-start.29 = (f32[512,8]{0,1:T(8,128)S(1)}, f32[512,8]{0,1:T(8,128)}, u32[]{:S(2)}) copy-start(f32[512,8]{0,1:T(8,128)} %param.29) | copy-start | bytes 49156
  7.2 29.6 %copy-start.11 = (bf16[512,512]{1,0:T(8,128)(2,1)S(1)}, bf16[512,512]{1,0:T(8,128)(2,1)}, u32[]{:S(2)}) copy-start(bf16[512,512]{1,0:T(8,128)(2,1)} %q_ref.1) | copy-start | bytes 1572868
  7.2 29.6 %copy-start.12 = (bf16[512,512]{1,0:T(8,128)(2,1)S(1)}, bf16[512,512]{1,0:T(8,128)(2,1)}, u32[]{:S(2)}) copy-start(bf16[512,512]{1,0:T(8,128)(2,1)} %k_ref.1) | copy-start | bytes 1572868
  7.2 29.6 %copy-start.13 = (bf16[512,512]{1,0:T(8,128)(2,1)S(1)}, bf16[512,512]{1,0:T(8,128)(2,1)}, u32[]{:S(2)}) copy-start(bf16[512,512]{1,0:T(8,128)(2,1)} %v_ref.1) | copy-start | bytes 1572868
  7.2 29.6 %copy-start.16 = (f32[512]{0:T(512)S(1)}, f32[512]{0:T(512)}, u32[]{:S(2)}) copy-start(f32[512]{0:T(512)} %param.27) | copy-start | bytes 6148
  7.2 29.6 %copy-start.17 = (f32[512]{0:T(512)S(1)}, f32[512]{0:T(512)}, u32[]{:S(2)}) copy-start(f32[512]{0:T(512)} %param.28) | copy-start | bytes 6148
  11.1 131.0 %all-to-all-start = ((bf16[32,16,1536]{2,1,0:T(8,128)(2,1)}), bf16[32,16,1536]{2,1,0:T(8,128)(2,1)S(1)}, u32[]{:S(2)}, u32[]{:S(2)}) async-start(bf16[32,16,1536]{2,1,0:T(8,128)(2,1)} %bitcast.22), calls=%async_computation | async-start | bytes 3145728 | tf_op jit(solution)/shard_map/all_to_all | solution.py:490
  36.6 189.3 %all-gather.3.cloned.1.call-start = ((), (), s32[]{:S(2)}) async-start(), calls=%async_computation.2 | async-start | bytes 4325376 | tf_op jit(solution)/shard_map/all_gather | solution.py:567
  36.9 1.0 copy-start.14
  37.9 1.0 copy-start.15
  66.3 26.1 %collective-permute-start.5 = (bf16[2048,256]{1,0:T(8,128)(2,1)}, bf16[2048,256]{1,0:T(8,128)(2,1)S(1)}, u32[]{:S(2)}, u32[]{:S(2)}) collective-permute-start(bf16[2048,256]{1,0:T(8,128)(2,1)} %bitcast.11.refs_3_), channel_id=1, source_target_pairs={{0,1},{1,2},{2,3},{3,0},{4,5},{5,6},{6,7},{7,4},{8,9},{9,10},{10,1... | collective-permute-start | bytes 3145736 | tf_op jit(solution)/shard_map/ppermute | solution.py:476
  67.8 47.0 %collective-permute-start.3 = (bf16[2048,256]{1,0:T(8,128)(2,1)}, bf16[2048,256]{1,0:T(8,128)(2,1)S(1)}, u32[]{:S(2)}, u32[]{:S(2)}) collective-permute-start(bf16[2048,256]{1,0:T(8,128)(2,1)} %bitcast.10.refs_2_), channel_id=1, source_target_pairs={{0,1},{1,2},{2,3},{3,0},{4,5},{5,6},{6,7},{7,4},{8,9},{9,10},{10,1... | collective-permute-start | bytes 3145736 | tf_op jit(solution)/shard_map/ppermute | solution.py:476
  69.1 47.8 %collective-permute-start.6 = (bf16[2048,256]{1,0:T(8,128)(2,1)}, bf16[2048,256]{1,0:T(8,128)(2,1)S(1)}, u32[]{:S(2)}, u32[]{:S(2)}) collective-permute-start(bf16[2048,256]{1,0:T(8,128)(2,1)} %bitcast.11.refs_3_), channel_id=1, source_target_pairs={{0,3},{1,0},{2,1},{3,2},{4,7},{5,4},{6,5},{7,6},{8,11},{9,8},{10,9... | collective-permute-start | bytes 3145736 | tf_op jit(solution)/shard_map/ppermute | solution.py:476
  70.5 46.5 %collective-permute-start.4 = (bf16[2048,256]{1,0:T(8,128)(2,1)}, bf16[2048,256]{1,0:T(8,128)(2,1)S(1)}, u32[]{:S(2)}, u32[]{:S(2)}) collective-permute-start(bf16[2048,256]{1,0:T(8,128)(2,1)} %bitcast.10.refs_2_), channel_id=1, source_target_pairs={{0,3},{1,0},{2,1},{3,2},{4,7},{5,4},{6,5},{7,6},{8,11},{9,8},{10,9... | collective-permute-start | bytes 3145736 | tf_op jit(solution)/shard_map/ppermute | solution.py:476
  70.9 66.5 %collective-permute-start.9 = (bf16[256,2048]{1,0:T(8,128)(2,1)}, bf16[256,2048]{1,0:T(8,128)(2,1)S(1)}, u32[]{:S(2)}, u32[]{:S(2)}) collective-permute-start(bf16[256,2048]{1,0:T(8,128)(2,1)} %bitcast.16), channel_id=1, source_target_pairs={{0,1},{1,2},{2,3},{3,0},{4,5},{5,6},{6,7},{7,4},{8,9},{9,10},{10,1... | collective-permute-start | bytes 3145736 | tf_op jit(solution)/shard_map/ppermute | solution.py:476
  92.5 45.8 %collective-permute-start.10 = (bf16[256,2048]{1,0:T(8,128)(2,1)}, bf16[256,2048]{1,0:T(8,128)(2,1)S(1)}, u32[]{:S(2)}, u32[]{:S(2)}) collective-permute-start(bf16[256,2048]{1,0:T(8,128)(2,1)} %bitcast.17), channel_id=1, source_target_pairs={{0,3},{1,0},{2,1},{3,2},{4,7},{5,4},{6,5},{7,6},{8,11},{9,8},{10,9... | collective-permute-start | bytes 3145736 | tf_op jit(solution)/shard_map/ppermute | solution.py:476
  117.0 54.6 %collective-permute-start.7 = (bf16[2048,256]{1,0:T(8,128)(2,1)}, bf16[2048,256]{1,0:T(8,128)(2,1)}, u32[]{:S(2)}, u32[]{:S(2)}) collective-permute-start(bf16[2048,256]{1,0:T(8,128)(2,1)} %pad_maximum_fusion), channel_id=1, source_target_pairs={{0,1},{1,2},{2,3},{3,0},{4,5},{5,6},{6,7},{7,4},{8,9},{9,10},{10,1... | collective-permute-start | bytes 3145736 | tf_op jit(solution)/shard_map/ppermute | solution.py:486
  117.0 1.4 copy-start.6
  117.0 21.2 %copy-start.8 = (bf16[2048,256]{1,0:T(8,128)(2,1)}, bf16[2048,256]{1,0:T(8,128)(2,1)S(1)}, u32[]{:S(2)}) copy-start(bf16[2048,256]{1,0:T(8,128)(2,1)S(1)} %collective-permute-done.4.refs_2_) | copy-start | bytes 3145732
  118.3 53.2 %collective-permute-start.8 = (bf16[2048,256]{1,0:T(8,128)(2,1)}, bf16[2048,256]{1,0:T(8,128)(2,1)}, u32[]{:S(2)}, u32[]{:S(2)}) collective-permute-start(bf16[2048,256]{1,0:T(8,128)(2,1)} %pad_maximum_fusion.1), channel_id=1, source_target_pairs={{0,3},{1,0},{2,1},{3,2},{4,7},{5,4},{6,5},{7,6},{8,11},{9,8},{10,9... | collective-permute-start | bytes 3145736 | tf_op jit(solution)/shard_map/ppermute | solution.py:486
  138.2 32.7 %collective-permute-start.11 = (bf16[128,2048]{1,0:T(8,128)(2,1)}, bf16[128,2048]{1,0:T(8,128)(2,1)S(1)}, u32[]{:S(2)}, u32[]{:S(2)}) collective-permute-start(bf16[128,2048]{1,0:T(8,128)(2,1)} %slice.36), channel_id=1, source_target_pairs={{0,1},{1,2},{2,3},{3,0},{4,5},{5,6},{6,7},{7,4},{8,9},{9,10},{10,1... | collective-permute-start | bytes 1572872 | tf_op jit(solution)/shard_map/ppermute | solution.py:486
  138.3 1.2 copy-start
  139.4 32.1 %collective-permute-start.12 = (bf16[128,2048]{1,0:T(8,128)(2,1)}, bf16[128,2048]{1,0:T(8,128)(2,1)}, u32[]{:S(2)}, u32[]{:S(2)}) collective-permute-start(bf16[128,2048]{1,0:T(8,128)(2,1)} %slice.37), channel_id=1, source_target_pairs={{0,3},{1,0},{2,1},{3,2},{4,7},{5,4},{6,5},{7,6},{8,11},{9,8},{10,9... | collective-permute-start | bytes 1572872 | tf_op jit(solution)/shard_map/ppermute | solution.py:486
  142.1 1.2 copy-start.3
  143.4 1.2 copy-start.5
  144.6 1.2 copy-start.7
  145.8 1.2 copy-start.9
  147.0 24.5 %copy-start.1 = (bf16[256,2048]{1,0:T(8,128)(2,1)S(1)}, bf16[256,2048]{1,0:T(8,128)(2,1)}, u32[]{:S(2)}) copy-start(bf16[256,2048]{1,0:T(8,128)(2,1)} %copy-done) | copy-start | bytes 3145732
  147.0 24.5 %copy-start.10 = (bf16[1,256,2048]{2,1,0:T(8,128)(2,1)S(1)}, bf16[1,256,2048]{2,1,0:T(8,128)(2,1)}, u32[]{:S(2)}) copy-start(bf16[1,256,2048]{2,1,0:T(8,128)(2,1)} %param.38) | copy-start | bytes 3145732
  180.0 14.3 %copy-start.23 = (bf16[128,2048]{1,0:T(8,128)(2,1)S(1)}, bf16[128,2048]{1,0:T(8,128)(2,1)}, u32[]{:S(2)}) copy-start(bf16[128,2048]{1,0:T(8,128)(2,1)} %get-tuple-element.31.refs_0_) | copy-start | bytes 1572868
  180.0 94.8 %all-to-all-start.1 = ((bf16[32,16,1536]{2,1,0:T(8,128)(2,1)}), bf16[32,16,1536]{2,1,0:T(8,128)(2,1)S(1)}, u32[]{:S(2)}, u32[]{:S(2)}) async-start(bf16[32,16,1536]{2,1,0:T(8,128)(2,1)} %bitcast.13), calls=%async_computation.1 | async-start | bytes 3145728 | tf_op jit(solution)/shard_map/all_to_all | solution.py:490
  194.3 14.1 %collective-permute-start.14 = (bf16[128,2048]{1,0:T(8,128)(2,1)S(1)}, bf16[128,2048]{1,0:T(8,128)(2,1)S(1)}, u32[]{:S(2)}, u32[]{:S(2)}) collective-permute-start(bf16[128,2048]{1,0:T(8,128)(2,1)S(1)} %copy-done.23), channel_id=1, source_target_pairs={{0,1},{1,2},{2,3},{3,0},{4,5},{5,6},{6,7},{7,4},{8,9},{9,10},{10,1... | collective-permute-start | bytes 1572872 | tf_op jit(solution)/shard_map/ppermute | solution.py:476
  195.5 13.7 %collective-permute-start.13 = (bf16[128,2048]{1,0:T(8,128)(2,1)S(1)}, bf16[128,2048]{1,0:T(8,128)(2,1)S(1)}, u32[]{:S(2)}, u32[]{:S(2)}) collective-permute-start(bf16[128,2048]{1,0:T(8,128)(2,1)S(1)} %copy-done.23), channel_id=1, source_target_pairs={{0,3},{1,0},{2,1},{3,2},{4,7},{5,4},{6,5},{7,6},{8,11},{9,8},{10,9... | collective-permute-start | bytes 1572872 | tf_op jit(solution)/shard_map/ppermute | solution.py:476
  208.4 8.5 %copy-start.21 = (bf16[128,2048]{1,0:T(8,128)(2,1)}, bf16[128,2048]{1,0:T(8,128)(2,1)S(1)}, u32[]{:S(2)}) copy-start(bf16[128,2048]{1,0:T(8,128)(2,1)S(1)} %collective-permute-done.14.refs_4_) | copy-start | bytes 1572868
  209.2 7.7 %collective-permute-start.15 = (bf16[64,2048]{1,0:T(8,128)(2,1)}, bf16[64,2048]{1,0:T(8,128)(2,1)S(1)}, u32[]{:S(2)}, u32[]{:S(2)}) collective-permute-start(bf16[64,2048]{1,0:T(8,128)(2,1)} %slice.38), channel_id=1, source_target_pairs={{0,1},{1,2},{2,3},{3,0},{4,5},{5,6},{6,7},{7,4},{8,9},{9,10},{10,1... | collective-permute-start | bytes 786440 | tf_op jit(solution)/shard_map/ppermute | solution.py:486
  209.2 7.7 %copy-start.22 = (bf16[128,2048]{1,0:T(8,128)(2,1)}, bf16[128,2048]{1,0:T(8,128)(2,1)S(1)}, u32[]{:S(2)}) copy-start(bf16[128,2048]{1,0:T(8,128)(2,1)S(1)} %collective-permute-done.13.refs_1_) | copy-start | bytes 1572868
  209.2 7.7 %collective-permute-start.16 = (bf16[64,2048]{1,0:T(8,128)(2,1)S(1)}, bf16[64,2048]{1,0:T(8,128)(2,1)S(1)}, u32[]{:S(2)}, u32[]{:S(2)}) collective-permute-start(bf16[64,2048]{1,0:T(8,128)(2,1)S(1)} %slice.39), channel_id=1, source_target_pairs={{0,3},{1,0},{2,1},{3,2},{4,7},{5,4},{6,5},{7,6},{8,11},{9,8},{10,9... | collective-permute-start | bytes 786440 | tf_op jit(solution)/shard_map/ppermute | solution.py:486
  223.1 18.3 %collective-permute-start.17 = (bf16[128,2048]{1,0:T(8,128)(2,1)}, bf16[128,2048]{1,0:T(8,128)(2,1)S(1)}, u32[]{:S(2)}, u32[]{:S(2)}) collective-permute-start(bf16[128,2048]{1,0:T(8,128)(2,1)} %get-tuple-element.33), channel_id=1, source_target_pairs={{0,1},{1,2},{2,3},{3,0},{4,5},{5,6},{6,7},{7,4},{8,9},{9,10},{10,1... | collective-permute-start | bytes 1572872 | tf_op jit(solution)/shard_map/ppermute | solution.py:472
  223.1 23.6 %collective-permute-start.18 = (bf16[128,2048]{1,0:T(8,128)(2,1)}, bf16[128,2048]{1,0:T(8,128)(2,1)S(1)}, u32[]{:S(2)}, u32[]{:S(2)}) collective-permute-start(bf16[128,2048]{1,0:T(8,128)(2,1)} %get-tuple-element.34), channel_id=1, source_target_pairs={{0,2},{1,3},{2,0},{3,1},{4,6},{5,7},{6,4},{7,5},{8,10},{9,11},{10,... | collective-permute-start | bytes 1572872 | tf_op jit(solution)/shard_map/ppermute | solution.py:472
  225.9 23.0 %collective-permute-start.19 = (bf16[128,2048]{1,0:T(8,128)(2,1)}, bf16[128,2048]{1,0:T(8,128)(2,1)}, u32[]{:S(2)}, u32[]{:S(2)}) collective-permute-start(bf16[128,2048]{1,0:T(8,128)(2,1)} %get-tuple-element.35), channel_id=1, source_target_pairs={{0,3},{1,0},{2,1},{3,2},{4,7},{5,4},{6,5},{7,6},{8,11},{9,8},{10,9... | collective-permute-start | bytes 1572872 | tf_op jit(solution)/shard_map/ppermute | solution.py:472
  229.3 12.1 %copy-start.30 = (f32[128,2]{0,1:T(2,128)S(1)}, f32[128,2]{0,1:T(2,128)}, u32[]{:S(2)}) copy-start(f32[128,2]{0,1:T(2,128)} %param.35) | copy-start | bytes 3076
  238.1 34.2 %copy-start.26 = (bf16[128,2048]{1,0:T(8,128)(2,1)S(1)}, bf16[128,2048]{1,0:T(8,128)(2,1)}, u32[]{:S(2)}) copy-start(bf16[128,2048]{1,0:T(8,128)(2,1)} %get-tuple-element.23) | copy-start | bytes 1572868
  238.1 24.2 %collective-permute-start.2 = (bf16[128,2048]{1,0:T(8,128)(2,1)}, bf16[128,2048]{1,0:T(8,128)(2,1)}, u32[]{:S(2)}, u32[]{:S(2)}) collective-permute-start(bf16[128,2048]{1,0:T(8,128)(2,1)} %get-tuple-element.26), channel_id=1, source_target_pairs={{0,3},{1,0},{2,1},{3,2},{4,7},{5,4},{6,5},{7,6},{8,11},{9,8},{10,9... | collective-permute-start | bytes 1572872 | tf_op jit(solution)/shard_map/ppermute | solution.py:472
  238.8 23.5 %collective-permute-start.1 = (bf16[128,2048]{1,0:T(8,128)(2,1)}, bf16[128,2048]{1,0:T(8,128)(2,1)}, u32[]{:S(2)}, u32[]{:S(2)}) collective-permute-start(bf16[128,2048]{1,0:T(8,128)(2,1)} %get-tuple-element.25), channel_id=1, source_target_pairs={{0,2},{1,3},{2,0},{3,1},{4,6},{5,7},{6,4},{7,5},{8,10},{9,11},{10,... | collective-permute-start | bytes 1572872 | tf_op jit(solution)/shard_map/ppermute | solution.py:472
  241.4 7.6 %copy-start.24 = (bf16[128,2048]{1,0:T(8,128)(2,1)}, bf16[128,2048]{1,0:T(8,128)(2,1)S(1)}, u32[]{:S(2)}) copy-start(bf16[128,2048]{1,0:T(8,128)(2,1)S(1)} %collective-permute-done.17.refs_3_) | copy-start | bytes 1572868
  241.4 30.9 %collective-permute-start = (bf16[128,2048]{1,0:T(8,128)(2,1)}, bf16[128,2048]{1,0:T(8,128)(2,1)}, u32[]{:S(2)}, u32[]{:S(2)}) collective-permute-start(bf16[128,2048]{1,0:T(8,128)(2,1)} %get-tuple-element.24), channel_id=1, source_target_pairs={{0,1},{1,2},{2,3},{3,0},{4,5},{5,6},{6,7},{7,4},{8,9},{9,10},{10,1... | collective-permute-start | bytes 1572872 | tf_op jit(solution)/shard_map/ppermute | solution.py:472
  246.7 2.3 copy-start.25
  274.8 1.2 copy-start.20
  (6 other events, 5.2 us)
Sparse Core Ops, SparseCore 0:
  66.5 87.9 all-gather.2

commit v2 on v1

--- a/solution.py
+++ b/solution.py
@@ -334,11 +334,12 @@
 
 
 def near_kernel(slot_rows, cap, r_ref, *refs):
-    *others, h_ref, x_ref = refs
-    count = len(others) // 2
+    *weights, x_ref, y_ref, h_ref = refs
+    count = len(weights) // 3
+    gates, ups, downs = weights[:count], weights[count : 2 * count], weights[2 * count :]
     total, main = r_ref.shape
     third = main // 3
-    ff = others[0].shape[1]
+    ff = gates[0].shape[1]
     size = min(256, total)
     kept = size // slot_rows * cap
     whole, tails = picks(size, slot_rows, cap)
@@ -351,41 +352,33 @@
             acc = acc + mm(tails[b], block[:, b * third : (b + 1) * third])
         x_ref[rows, main:] = acc.astype(BF16)
     for k in range(count):
-        gate = mm(x_ref[...], others[k][...])
-        up = mm(x_ref[...], others[count + k][...])
+        gate = mm(x_ref[...], gates[k][...])
+        up = mm(x_ref[...], ups[k][...])
         h_ref[:, k * ff : (k + 1) * ff] = (gate * sigmoid(gate) * up).astype(BF16)
-
-
-def far_kernel(slot_rows, cap, x_ref, h_ref, gate_ref, up_ref, fa_ref, fb_ref, *refs):
-    *downs, o_ref, f_ref, tail_ref = refs
+    for b in range(4):
+        cols = slice(b * third, (b + 1) * third)
+        acc = mm(h_ref[:, :ff], downs[0][:, cols])
+        for k in range(1, count):
+            acc = acc + mm(h_ref[:, k * ff : (k + 1) * ff], downs[k][:, cols])
+        y_ref[:, cols] = acc
+
+
+def far_kernel(slot_rows, cap, x_ref, y_ref, fa_ref, fb_ref, da_ref, db_ref, o_ref, f_ref, tail_ref):
     total, main = o_ref.shape
     third = main // 3
     half = fa_ref.shape[0] // 2
-    ff = gate_ref.shape[1]
+    low_ff = da_ref.shape[0]
     size = min(256, total)
     kept = size // slot_rows * cap
     whole, tails = picks(size, slot_rows, cap)
-    gate = mm(x_ref[...], gate_ref[...])
-    up = mm(x_ref[...], up_ref[...])
-    f_ref[:, :ff] = (gate * sigmoid(gate) * up).astype(BF16)
     low, high = x_ref[:, :half], x_ref[:, half:]
     gate = mm(low, fa_ref[:half]) + mm(high, fb_ref[:half])
     up = mm(low, fa_ref[half:]) + mm(high, fb_ref[half:])
-    f_ref[:, ff:] = (gate * sigmoid(gate) * up).astype(BF16)
+    f_ref[...] = (gate * sigmoid(gate) * up).astype(BF16)
 
     def lower(cols):
-        acc = None
-        at = 0
-        for d_ref in downs:
-            count = d_ref.shape[0]
-            if at < h_ref.shape[1]:
-                h = h_ref[:, at : at + count]
-            else:
-                h = f_ref[:, at - h_ref.shape[1] : at - h_ref.shape[1] + count]
-            part = mm(h, d_ref[:, cols])
-            acc = part if acc is None else acc + part
-            at += count
-        return acc.astype(BF16)
+        far = mm(f_ref[:, :low_ff], da_ref[:, cols]) + mm(f_ref[:, low_ff:], db_ref[:, cols])
+        return (y_ref[:, cols] + far).astype(BF16)
 
     tail_ref[...] = lower(slice(main, main + third))
     for b in range(3):
@@ -569,26 +562,26 @@
 
     in_vmem = pl.BlockSpec(memory_space=pltpu.MemorySpace.VMEM)
     kept = experts * cap
-    hidden, rows = pl.pallas_call(
+    rows, part = pl.pallas_call(
         bind(near_kernel, slot_rows, cap),
-        in_specs=[in_vmem] * 5,
+        in_specs=[in_vmem] * 10,
         out_specs=[in_vmem] * 2,
         out_shape=[
-            jax.ShapeDtypeStruct((kept, 2 * ff), BF16),
             jax.ShapeDtypeStruct((kept, model), BF16),
+            jax.ShapeDtypeStruct((kept, model), F32),
         ],
+        scratch_shapes=[pltpu.VMEM((kept, 3 * ff), BF16)],
         compiler_params=params(SMALL_LIMIT),
         name="near",
-    )(received, *gate_near, *up_near)
-    downs = (*down_near, down_own, *down_far)
+    )(received, gate_own, *gate_near, up_own, *up_near, down_own, *down_near)
     returning = pl.pallas_call(
         bind(far_kernel, slot_rows, cap),
-        in_specs=[in_vmem] * (6 + len(downs)),
+        in_specs=[in_vmem] * 6,
         out_shape=jax.ShapeDtypeStruct((total, main), BF16),
-        scratch_shapes=[pltpu.VMEM((kept, 2 * ff), BF16), pltpu.VMEM((kept, third), BF16)],
+        scratch_shapes=[pltpu.VMEM((kept, ff), BF16), pltpu.VMEM((kept, third), BF16)],
         compiler_params=params(SMALL_LIMIT),
         name="far",
-    )(rows, hidden, gate_own, up_own, *both_far, *downs)
+    )(rows, part, *both_far, *down_far)
     expert_out = exchange(returning.reshape(experts, slot_rows, main), "ep").reshape(total, main)
 
     shared_part = pl.pallas_call(

time: 287 us -> 285 us (level)
  waiting for transfers between devices: 122 us -> 116 us
  local copies, waits for them, and re-layouts: 17.3 us -> 21.2 us
    ppermute x3, waiting for transfers between devices: 26.4 us -> 19.5 us  [from_far(): lax.ppermute(low, axis, ring(axis, 1))]
    unnamed x64 -> x68, local copies, waits for them, and re-layouts: 14.5 us -> 18.4 us
where the time goes in v2:
time: 285 us; the launch traced here: 284 us
  waiting for transfers between devices  116 us (41%)
  starting transfers between devices  63.6 us (22%)
  Pallas kernels  63.5 us (22%)
  local copies, waits for them, and re-layouts  21.2 us (7%)
  between operations  14.3 us (5%)
  other arithmetic  4.8 us (2%)
    ppermute x4, waiting for transfers between devices, from_near(): lax.ppermute(x, axis, ring(axis, 1))  69.2 us
    all_to_all x2, starting transfers between devices, exchange(): return lax.all_to_all(x, axis, split_axis=0, concat_axis=0, tiled=True)  39.7 us
    ppermute x6, waiting for transfers between devices, turn_exchange(): lax.ppermute(blocks[d], axis, ring(axis, d))  26.8 us
    pallas_call x1, Pallas kernels, run_mixer_local(): pl.pallas_call(mixer_local, grid=(pairs,), in_specs=[spec] * 5 + [pl.Bloc...  25.5 us
    ppermute x3, waiting for transfers between devices, from_far(): lax.ppermute(low, axis, ring(axis, 1))  19.5 us
    unnamed x68, local copies, waits for them, and re-layouts  18.4 us
    pallas_call x1, Pallas kernels, run_mixer_final(): pl.pallas_call(mixer_final, grid_spec=pltpu.PrefetchScalarGridSpec(num_sc...  8.78 us
    ppermute x3, starting transfers between devices, from_far(): lax.ppermute(high, axis, ring(axis, -1))  8.13 us
  transfers between devices with their start and end apart: 23, of which 11 were waited for; matrix products, arithmetic and copies ran while one was open for 3% of the time, Pallas kernels for 20%

profile of v2, /device:TPU:33, one launch (start us, length us, event | category | flops | bytes accessed | tf_op | source)
XLA Modules:
  0.0 283.6 jit_solution(10210597267329201306)
XLA Ops:
  7.2 3.9 %dispatch.1 = (bf16[128,2048]{1,0:T(8,128)(2,1)}, bf16[512,1536]{1,0:T(8,128)(2,1)}, s32[128,2]{1,0:T(8,128)}) custom-call(bf16[128,2048]{1,0:T(8,128)(2,1)} %refs_0_.1, f32[1,2048]{1,0:T(1,128)} %bitcast.29, s32[2,128]{1,0:T(2,128)} %bitcast.30), custom_call_target="tpu_custom_call" | custom-call | tf_op jit(solution)/shard_map/dispatch/pallas_call | solution.py:534
  11.2 25.5 %all-to-all-start = ((bf16[32,16,1536]{2,1,0:T(8,128)(2,1)}), bf16[32,16,1536]{2,1,0:T(8,128)(2,1)S(1)}, u32[]{:S(2)}, u32[]{:S(2)}) async-start(bf16[32,16,1536]{2,1,0:T(8,128)(2,1)} %bitcast.28), calls=%async_computation | async-start | bytes 3145728 | tf_op jit(solution)/shard_map/all_to_all | solution.py:483
  36.9 1.0 copy-done.16
  37.9 1.0 copy-done.17
  39.0 25.5 %mixer_local.1 = (f32[512,512]{1,0:T(8,128)S(1)}, bf16[512,512]{1,0:T(8,128)(2,1)S(1)}, bf16[512,128]{1,0:T(8,128)(2,1)}) custom-call(bf16[512,512]{1,0:T(8,128)(2,1)S(1)} %copy-done.13, bf16[512,512]{1,0:T(8,128)(2,1)S(1)} %copy-done.14, bf16[512,512]{1,0:T(8,128)(2,1)S(1)} %copy-done.15, bf16[512,512]{1,0:T(8,128)(2,1)S(1)} %copy-done.16, ...), custom_call_target="tpu_custom_call" | custom-call | flops 40000000000 | bytes 5000000 | tf_op jit(solution)/shard_map/mixer_local/pallas_call | solution.py:161
  66.3 1.5 collective-permute-start.5
  67.8 1.3 collective-permute-start.3
  69.1 1.3 collective-permute-start.6
  70.9 1.0 collective-permute-start.7
  71.9 20.5 %collective-permute-done.5.refs_5_ = bf16[2048,256]{1,0:T(8,128)(2,1)S(1)} collective-permute-done((bf16[2048,256]{1,0:T(8,128)(2,1)}, bf16[2048,256]{1,0:T(8,128)(2,1)S(1)}, u32[]{:S(2)}, u32[]{:S(2)}) %collective-permute-start.5) | collective-permute-done | bytes 1048608 | tf_op jit(solution)/shard_map/ppermute | solution.py:469
  92.4 1.2 collective-permute-start.8
  93.7 21.1 %collective-permute-done.3.refs_2_ = bf16[2048,256]{1,0:T(8,128)(2,1)S(1)} collective-permute-done((bf16[2048,256]{1,0:T(8,128)(2,1)}, bf16[2048,256]{1,0:T(8,128)(2,1)S(1)}, u32[]{:S(2)}, u32[]{:S(2)}) %collective-permute-start.3) | collective-permute-done | bytes 1048608 | tf_op jit(solution)/shard_map/ppermute | solution.py:469
  114.9 1.0 copy-done
  115.9 1.1 pad_maximum_fusion
  117.1 1.2 pad_maximum_fusion.1
  118.3 2.7 collective-permute-start.10
  121.0 16.3 %collective-permute-done.7.refs_8_ = bf16[256,2048]{1,0:T(8,128)(2,1)S(1)} collective-permute-done((bf16[256,2048]{1,0:T(8,128)(2,1)}, bf16[256,2048]{1,0:T(8,128)(2,1)S(1)}, u32[]{:S(2)}, u32[]{:S(2)}) %collective-permute-start.7) | collective-permute-done | bytes 1048608 | tf_op jit(solution)/shard_map/ppermute | solution.py:469
  139.4 2.7 collective-permute-start.12
  142.1 1.2 copy-done.1
  143.3 1.2 copy-done.3
  144.5 1.2 copy-done.5
  145.8 1.2 copy-done.7
  147.0 1.2 copy-done.9
  148.2 1.2 copy-done.10
  149.5 1.2 copy-done.11
  150.7 1.2 copy-done.12
  151.9 4.5 %near.1 = (bf16[384,2048]{1,0:T(8,128)(2,1)S(1)}, f32[384,2048]{1,0:T(8,128)S(1)}) custom-call(bf16[512,1536]{1,0:T(8,128)(2,1)S(1)} %bitcast.15, bf16[2048,256]{1,0:T(8,128)(2,1)S(1)} %bitcast.18, bf16[2048,256]{1,0:T(8,128)(2,1)S(1)} %copy-done.1, bf16[2048,256]{1,0:T(8,128)(2,1)S(1)} %copy-done.5, bf16[2048,256]{1,0:T(8,128)(2,1)S(1)} %bitcast.21, ...), custom_call_target="tpu_custom_call" | custom-call | tf_op jit(solution)/shard_map/near/pallas_call | solution.py:565
  156.4 14.6 %collective-permute-done.11.refs_4_ = bf16[128,2048]{1,0:T(8,128)(2,1)S(1)} collective-permute-done((bf16[128,2048]{1,0:T(8,128)(2,1)}, bf16[128,2048]{1,0:T(8,128)(2,1)S(1)}, u32[]{:S(2)}, u32[]{:S(2)}) %collective-permute-start.11) | collective-permute-done | bytes 524320 | tf_op jit(solution)/shard_map/ppermute | solution.py:479
  171.6 5.9 %far.1 = bf16[512,1536]{1,0:T(8,128)(2,1)} custom-call(bf16[384,2048]{1,0:T(8,128)(2,1)S(1)} %get-tuple-element.28.refs_0_, f32[384,2048]{1,0:T(8,128)S(1)} %get-tuple-element.29.refs_1_, bf16[2048,256]{1,0:T(8,128)(2,1)} %collective-permute-done.9.refs_2_, bf16[2048,256]{1,0:T(8,128)(2,1)} %collective-permute-done.10.refs_3_, ...), custom_call_target="tpu_custom_call" | custom-call | tf_op jit(solution)/shard_map/far/pallas_call | solution.py:577
  177.5 14.3 %all-to-all-start.1 = ((bf16[32,16,1536]{2,1,0:T(8,128)(2,1)}), bf16[32,16,1536]{2,1,0:T(8,128)(2,1)S(1)}, u32[]{:S(2)}, u32[]{:S(2)}) async-start(bf16[32,16,1536]{2,1,0:T(8,128)(2,1)} %bitcast.13), calls=%async_computation.1 | async-start | bytes 3145728 | tf_op jit(solution)/shard_map/all_to_all | solution.py:483
  191.8 1.2 collective-permute-start.14
  193.0 1.6 collective-permute-start.13
  194.6 11.3 %collective-permute-done.14.refs_4_ = bf16[128,2048]{1,0:T(8,128)(2,1)S(1)} collective-permute-done((bf16[128,2048]{1,0:T(8,128)(2,1)S(1)}, bf16[128,2048]{1,0:T(8,128)(2,1)S(1)}, u32[]{:S(2)}, u32[]{:S(2)}) %collective-permute-start.14) | collective-permute-done | bytes 524320 | tf_op jit(solution)/shard_map/ppermute | solution.py:469
  206.7 2.8 collective-permute-start.16
  209.5 4.9 %collective-permute-done.15.refs_2_ = bf16[64,2048]{1,0:T(8,128)(2,1)S(1)} collective-permute-done((bf16[64,2048]{1,0:T(8,128)(2,1)}, bf16[64,2048]{1,0:T(8,128)(2,1)S(1)}, u32[]{:S(2)}, u32[]{:S(2)}) %collective-permute-start.15) | collective-permute-done | bytes 262176 | tf_op jit(solution)/shard_map/ppermute | solution.py:479
  215.8 4.7 %shared.1 = (bf16[128,2048]{1,0:T(8,128)(2,1)}, bf16[128,2048]{1,0:T(8,128)(2,1)}, bf16[128,2048]{1,0:T(8,128)(2,1)}, bf16[128,2048]{1,0:T(8,128)(2,1)}) custom-call(bf16[128,2048]{1,0:T(8,128)(2,1)} %get-tuple-element.31.refs_0_, bf16[128,2048]{1,0:T(8,128)(2,1)} %copy-done.24, bf16[64,2048]{1,0:T(8,128)(2,1)} %copy-done.29, bf16[64,2048]{1,0:T(8,128)(2,1)} %copy-done.30, ...), custom_call_target="tpu_custom_call" | custom-call | tf_op jit(solution)/shard_map/shared/pallas_call | solution.py:587
  220.6 2.8 collective-permute-start.18
  223.4 3.4 %chain.1.s_ref = bf16[256,128]{1,0:T(8,128)(2,1)} custom-call(s32[1]{0:T(128)} %bitcast.3.me_ref, bf16[32,512,128]{2,1,0:T(8,128)(2,1)} %bitcast.31), custom_call_target="tpu_custom_call" | custom-call | flops 3000000000 | bytes 4000000 | tf_op jit(solution)/shard_map/chain/pallas_call | solution.py:208
  226.8 8.8 %mixer_final.1 = (bf16[128,2048]{1,0:T(8,128)(2,1)}, bf16[128,2048]{1,0:T(8,128)(2,1)}, bf16[128,2048]{1,0:T(8,128)(2,1)}, bf16[128,2048]{1,0:T(8,128)(2,1)}) custom-call(s32[1]{0:T(128)} %bitcast.me_ref, f32[512,512]{1,0:T(8,128)} %copy-done.20, bf16[512,512]{1,0:T(8,128)(2,1)} %copy-done.21, bf16[256,128]{1,0:T(8,128)(2,1)} %chain.1.s_ref, ...), custom_call_target="tpu_custom_call" | custom-call | flops 6000000000 | bytes 8000000 | tf_op jit(solution)/shard_map/mixer_final/pallas_call | solution.py:267
  236.2 2.6 collective-permute-start.1
  239.6 4.5 %collective-permute-done.18.refs_4_ = bf16[128,2048]{1,0:T(8,128)(2,1)S(1)} collective-permute-done((bf16[128,2048]{1,0:T(8,128)(2,1)}, bf16[128,2048]{1,0:T(8,128)(2,1)S(1)}, u32[]{:S(2)}, u32[]{:S(2)}) %collective-permute-start.18) | collective-permute-done | bytes 524320 | tf_op jit(solution)/shard_map/ppermute | solution.py:465
  244.1 2.3 collective-permute-done.19.refs_5_
  246.4 3.4 %prepare.1 = (bf16[768,512]{1,0:T(8,128)(2,1)}, f32[128,2048]{1,0:T(8,128)}) custom-call(s32[128,2]{1,0:T(8,128)} %get-tuple-element.30.refs_0_, f32[128,2]{1,0:T(8,128)} %copy.24.refs_1_, bf16[128,2048]{1,0:T(8,128)(2,1)} %get-tuple-element.32.refs_2_, bf16[128,2048]{1,0:T(8,128)(2,1)} %copy-done.26, bf16[128,2048]{1,0:T(8,128)(2,1)} %copy-done.27, ...), custom_call_target="tpu_custom_call" | custom-call | tf_op jit(solution)/shard_map/prepare/pallas_call | solution.py:618
  249.8 10.0 %collective-permute-done.2 = bf16[128,2048]{1,0:T(8,128)(2,1)} collective-permute-done((bf16[128,2048]{1,0:T(8,128)(2,1)}, bf16[128,2048]{1,0:T(8,128)(2,1)}, u32[]{:S(2)}, u32[]{:S(2)}) %collective-permute-start.2) | collective-permute-done | bytes 524320 | tf_op jit(solution)/shard_map/ppermute | solution.py:465
  259.8 10.0 %collective-permute-done = bf16[128,2048]{1,0:T(8,128)(2,1)} collective-permute-done((bf16[128,2048]{1,0:T(8,128)(2,1)}, bf16[128,2048]{1,0:T(8,128)(2,1)}, u32[]{:S(2)}, u32[]{:S(2)}) %collective-permute-start) | collective-permute-done | bytes 524320 | tf_op jit(solution)/shard_map/ppermute | solution.py:465
  269.8 2.5 add_convert_fusion
  272.3 1.2 copy-done.22
  273.4 3.3 %combine.1 = bf16[128,2048]{1,0:T(8,128)(2,1)} custom-call(bf16[512,1536]{1,0:T(8,128)(2,1)} %bitcast.27, bf16[768,512]{1,0:T(8,128)(2,1)} %get-tuple-element.36.w_ref, f32[128,2048]{1,0:T(8,128)} %get-tuple-element.37.base_ref), custom_call_target="tpu_custom_call" | custom-call | tf_op jit(solution)/shard_map/combine/pallas_call | solution.py:627
  (87 shorter events, 9.1 us)
Async XLA Ops:
  7.2 29.5 %copy-start.31 = (f32[512,8]{0,1:T(8,128)S(1)}, f32[512,8]{0,1:T(8,128)}, u32[]{:S(2)}) copy-start(f32[512,8]{0,1:T(8,128)} %param.29) | copy-start | bytes 49156
  7.2 29.7 %copy-start.13 = (bf16[512,512]{1,0:T(8,128)(2,1)S(1)}, bf16[512,512]{1,0:T(8,128)(2,1)}, u32[]{:S(2)}) copy-start(bf16[512,512]{1,0:T(8,128)(2,1)} %q_ref.1) | copy-start | bytes 1572868
  7.2 29.7 %copy-start.14 = (bf16[512,512]{1,0:T(8,128)(2,1)S(1)}, bf16[512,512]{1,0:T(8,128)(2,1)}, u32[]{:S(2)}) copy-start(bf16[512,512]{1,0:T(8,128)(2,1)} %k_ref.1) | copy-start | bytes 1572868
  7.2 29.7 %copy-start.15 = (bf16[512,512]{1,0:T(8,128)(2,1)S(1)}, bf16[512,512]{1,0:T(8,128)(2,1)}, u32[]{:S(2)}) copy-start(bf16[512,512]{1,0:T(8,128)(2,1)} %v_ref.1) | copy-start | bytes 1572868
  7.2 29.7 %copy-start.18 = (f32[512]{0:T(512)S(1)}, f32[512]{0:T(512)}, u32[]{:S(2)}) copy-start(f32[512]{0:T(512)} %param.27) | copy-start | bytes 6148
  7.2 29.7 %copy-start.19 = (f32[512]{0:T(512)S(1)}, f32[512]{0:T(512)}, u32[]{:S(2)}) copy-start(f32[512]{0:T(512)} %param.28) | copy-start | bytes 6148
  11.2 130.9 %all-to-all-start = ((bf16[32,16,1536]{2,1,0:T(8,128)(2,1)}), bf16[32,16,1536]{2,1,0:T(8,128)(2,1)S(1)}, u32[]{:S(2)}, u32[]{:S(2)}) async-start(bf16[32,16,1536]{2,1,0:T(8,128)(2,1)} %bitcast.28), calls=%async_computation | async-start | bytes 3145728 | tf_op jit(solution)/shard_map/all_to_all | solution.py:483
  36.6 186.7 %all-gather.3.cloned.1.call-start = ((), (), s32[]{:S(2)}) async-start(), calls=%async_computation.2 | async-start | bytes 4325376 | tf_op jit(solution)/shard_map/all_gather | solution.py:560
  66.3 26.1 %collective-permute-start.5 = (bf16[2048,256]{1,0:T(8,128)(2,1)}, bf16[2048,256]{1,0:T(8,128)(2,1)S(1)}, u32[]{:S(2)}, u32[]{:S(2)}) collective-permute-start(bf16[2048,256]{1,0:T(8,128)(2,1)} %bitcast.19), channel_id=1, source_target_pairs={{0,1},{1,2},{2,3},{3,0},{4,5},{5,6},{6,7},{7,4},{8,9},{9,10},{10,1... | collective-permute-start | bytes 3145736 | tf_op jit(solution)/shard_map/ppermute | solution.py:469
  67.8 47.0 %collective-permute-start.3 = (bf16[2048,256]{1,0:T(8,128)(2,1)}, bf16[2048,256]{1,0:T(8,128)(2,1)S(1)}, u32[]{:S(2)}, u32[]{:S(2)}) collective-permute-start(bf16[2048,256]{1,0:T(8,128)(2,1)} %bitcast.16), channel_id=1, source_target_pairs={{0,1},{1,2},{2,3},{3,0},{4,5},{5,6},{6,7},{7,4},{8,9},{9,10},{10,1... | collective-permute-start | bytes 3145736 | tf_op jit(solution)/shard_map/ppermute | solution.py:469
  69.1 47.8 %collective-permute-start.6 = (bf16[2048,256]{1,0:T(8,128)(2,1)}, bf16[2048,256]{1,0:T(8,128)(2,1)S(1)}, u32[]{:S(2)}, u32[]{:S(2)}) collective-permute-start(bf16[2048,256]{1,0:T(8,128)(2,1)} %bitcast.20), channel_id=1, source_target_pairs={{0,3},{1,0},{2,1},{3,2},{4,7},{5,4},{6,5},{7,6},{8,11},{9,8},{10,9... | collective-permute-start | bytes 3145736 | tf_op jit(solution)/shard_map/ppermute | solution.py:469
  70.5 46.5 %collective-permute-start.4 = (bf16[2048,256]{1,0:T(8,128)(2,1)}, bf16[2048,256]{1,0:T(8,128)(2,1)S(1)}, u32[]{:S(2)}, u32[]{:S(2)}) collective-permute-start(bf16[2048,256]{1,0:T(8,128)(2,1)} %bitcast.17), channel_id=1, source_target_pairs={{0,3},{1,0},{2,1},{3,2},{4,7},{5,4},{6,5},{7,6},{8,11},{9,8},{10,9... | collective-permute-start | bytes 3145736 | tf_op jit(solution)/shard_map/ppermute | solution.py:469
  70.9 66.4 %collective-permute-start.7 = (bf16[256,2048]{1,0:T(8,128)(2,1)}, bf16[256,2048]{1,0:T(8,128)(2,1)S(1)}, u32[]{:S(2)}, u32[]{:S(2)}) collective-permute-start(bf16[256,2048]{1,0:T(8,128)(2,1)} %bitcast.22), channel_id=1, source_target_pairs={{0,1},{1,2},{2,3},{3,0},{4,5},{5,6},{6,7},{7,4},{8,9},{9,10},{10,1... | collective-permute-start | bytes 3145736 | tf_op jit(solution)/shard_map/ppermute | solution.py:469
  92.4 45.8 %collective-permute-start.8 = (bf16[256,2048]{1,0:T(8,128)(2,1)}, bf16[256,2048]{1,0:T(8,128)(2,1)S(1)}, u32[]{:S(2)}, u32[]{:S(2)}) collective-permute-start(bf16[256,2048]{1,0:T(8,128)(2,1)} %bitcast.23), channel_id=1, source_target_pairs={{0,3},{1,0},{2,1},{3,2},{4,7},{5,4},{6,5},{7,6},{8,11},{9,8},{10,9... | collective-permute-start | bytes 3145736 | tf_op jit(solution)/shard_map/ppermute | solution.py:469
  117.0 54.6 %collective-permute-start.9 = (bf16[2048,256]{1,0:T(8,128)(2,1)}, bf16[2048,256]{1,0:T(8,128)(2,1)}, u32[]{:S(2)}, u32[]{:S(2)}) collective-permute-start(bf16[2048,256]{1,0:T(8,128)(2,1)} %pad_maximum_fusion), channel_id=1, source_target_pairs={{0,1},{1,2},{2,3},{3,0},{4,5},{5,6},{6,7},{7,4},{8,9},{9,10},{10,1... | collective-permute-start | bytes 3145736 | tf_op jit(solution)/shard_map/ppermute | solution.py:479
  117.0 1.4 copy-start.2
  117.0 21.2 %copy-start.4 = (bf16[2048,256]{1,0:T(8,128)(2,1)}, bf16[2048,256]{1,0:T(8,128)(2,1)S(1)}, u32[]{:S(2)}) copy-start(bf16[2048,256]{1,0:T(8,128)(2,1)S(1)} %collective-permute-done.4.refs_3_) | copy-start | bytes 3145732
  118.3 53.2 %collective-permute-start.10 = (bf16[2048,256]{1,0:T(8,128)(2,1)}, bf16[2048,256]{1,0:T(8,128)(2,1)}, u32[]{:S(2)}, u32[]{:S(2)}) collective-permute-start(bf16[2048,256]{1,0:T(8,128)(2,1)} %pad_maximum_fusion.1), channel_id=1, source_target_pairs={{0,3},{1,0},{2,1},{3,2},{4,7},{5,4},{6,5},{7,6},{8,11},{9,8},{10,9... | collective-permute-start | bytes 3145736 | tf_op jit(solution)/shard_map/ppermute | solution.py:479
  137.3 1.9 copy-start.6
  138.2 32.8 %collective-permute-start.11 = (bf16[128,2048]{1,0:T(8,128)(2,1)}, bf16[128,2048]{1,0:T(8,128)(2,1)S(1)}, u32[]{:S(2)}, u32[]{:S(2)}) collective-permute-start(bf16[128,2048]{1,0:T(8,128)(2,1)} %slice.36), channel_id=1, source_target_pairs={{0,1},{1,2},{2,3},{3,0},{4,5},{5,6},{6,7},{7,4},{8,9},{9,10},{10,1... | collective-permute-start | bytes 1572872 | tf_op jit(solution)/shard_map/ppermute | solution.py:479
  139.4 32.1 %collective-permute-start.12 = (bf16[128,2048]{1,0:T(8,128)(2,1)}, bf16[128,2048]{1,0:T(8,128)(2,1)}, u32[]{:S(2)}, u32[]{:S(2)}) collective-permute-start(bf16[128,2048]{1,0:T(8,128)(2,1)} %slice.37), channel_id=1, source_target_pairs={{0,3},{1,0},{2,1},{3,2},{4,7},{5,4},{6,5},{7,6},{8,11},{9,8},{10,9... | collective-permute-start | bytes 1572872 | tf_op jit(solution)/shard_map/ppermute | solution.py:479
  142.1 1.2 copy-start.1
  143.3 1.2 copy-start.3
  144.5 1.2 copy-start.5
  145.8 1.2 copy-start.7
  147.0 1.2 copy-start.9
  148.2 1.2 copy-start.10
  149.4 1.2 copy-start.11
  150.7 1.2 copy-start.12
  177.5 14.3 %copy-start.25 = (bf16[128,2048]{1,0:T(8,128)(2,1)S(1)}, bf16[128,2048]{1,0:T(8,128)(2,1)}, u32[]{:S(2)}) copy-start(bf16[128,2048]{1,0:T(8,128)(2,1)} %get-tuple-element.31.refs_0_) | copy-start | bytes 1572868
  177.5 94.7 %all-to-all-start.1 = ((bf16[32,16,1536]{2,1,0:T(8,128)(2,1)}), bf16[32,16,1536]{2,1,0:T(8,128)(2,1)S(1)}, u32[]{:S(2)}, u32[]{:S(2)}) async-start(bf16[32,16,1536]{2,1,0:T(8,128)(2,1)} %bitcast.13), calls=%async_computation.1 | async-start | bytes 3145728 | tf_op jit(solution)/shard_map/all_to_all | solution.py:483
  191.8 14.1 %collective-permute-start.14 = (bf16[128,2048]{1,0:T(8,128)(2,1)S(1)}, bf16[128,2048]{1,0:T(8,128)(2,1)S(1)}, u32[]{:S(2)}, u32[]{:S(2)}) collective-permute-start(bf16[128,2048]{1,0:T(8,128)(2,1)S(1)} %copy-done.25), channel_id=1, source_target_pairs={{0,1},{1,2},{2,3},{3,0},{4,5},{5,6},{6,7},{7,4},{8,9},{9,10},{10,1... | collective-permute-start | bytes 1572872 | tf_op jit(solution)/shard_map/ppermute | solution.py:469
  193.0 13.7 %collective-permute-start.13 = (bf16[128,2048]{1,0:T(8,128)(2,1)S(1)}, bf16[128,2048]{1,0:T(8,128)(2,1)S(1)}, u32[]{:S(2)}, u32[]{:S(2)}) collective-permute-start(bf16[128,2048]{1,0:T(8,128)(2,1)S(1)} %copy-done.25), channel_id=1, source_target_pairs={{0,3},{1,0},{2,1},{3,2},{4,7},{5,4},{6,5},{7,6},{8,11},{9,8},{10,9... | collective-permute-start | bytes 1572872 | tf_op jit(solution)/shard_map/ppermute | solution.py:469
  205.9 8.5 %copy-start.23 = (bf16[128,2048]{1,0:T(8,128)(2,1)}, bf16[128,2048]{1,0:T(8,128)(2,1)S(1)}, u32[]{:S(2)}) copy-start(bf16[128,2048]{1,0:T(8,128)(2,1)S(1)} %collective-permute-done.14.refs_4_) | copy-start | bytes 1572868
  206.7 7.7 %collective-permute-start.15 = (bf16[64,2048]{1,0:T(8,128)(2,1)}, bf16[64,2048]{1,0:T(8,128)(2,1)S(1)}, u32[]{:S(2)}, u32[]{:S(2)}) collective-permute-start(bf16[64,2048]{1,0:T(8,128)(2,1)} %slice.38), channel_id=1, source_target_pairs={{0,1},{1,2},{2,3},{3,0},{4,5},{5,6},{6,7},{7,4},{8,9},{9,10},{10,1... | collective-permute-start | bytes 786440 | tf_op jit(solution)/shard_map/ppermute | solution.py:479
  206.7 7.7 %copy-start.24 = (bf16[128,2048]{1,0:T(8,128)(2,1)}, bf16[128,2048]{1,0:T(8,128)(2,1)S(1)}, u32[]{:S(2)}) copy-start(bf16[128,2048]{1,0:T(8,128)(2,1)S(1)} %collective-permute-done.13.refs_1_) | copy-start | bytes 1572868
  206.7 7.7 %collective-permute-start.16 = (bf16[64,2048]{1,0:T(8,128)(2,1)S(1)}, bf16[64,2048]{1,0:T(8,128)(2,1)S(1)}, u32[]{:S(2)}, u32[]{:S(2)}) collective-permute-start(bf16[64,2048]{1,0:T(8,128)(2,1)S(1)} %slice.39), channel_id=1, source_target_pairs={{0,3},{1,0},{2,1},{3,2},{4,7},{5,4},{6,5},{7,6},{8,11},{9,8},{10,9... | collective-permute-start | bytes 786440 | tf_op jit(solution)/shard_map/ppermute | solution.py:479
  220.6 18.3 %collective-permute-start.17 = (bf16[128,2048]{1,0:T(8,128)(2,1)}, bf16[128,2048]{1,0:T(8,128)(2,1)S(1)}, u32[]{:S(2)}, u32[]{:S(2)}) collective-permute-start(bf16[128,2048]{1,0:T(8,128)(2,1)} %get-tuple-element.33), channel_id=1, source_target_pairs={{0,1},{1,2},{2,3},{3,0},{4,5},{5,6},{6,7},{7,4},{8,9},{9,10},{10,1... | collective-permute-start | bytes 1572872 | tf_op jit(solution)/shard_map/ppermute | solution.py:465
  220.6 23.6 %collective-permute-start.18 = (bf16[128,2048]{1,0:T(8,128)(2,1)}, bf16[128,2048]{1,0:T(8,128)(2,1)S(1)}, u32[]{:S(2)}, u32[]{:S(2)}) collective-permute-start(bf16[128,2048]{1,0:T(8,128)(2,1)} %get-tuple-element.34), channel_id=1, source_target_pairs={{0,2},{1,3},{2,0},{3,1},{4,6},{5,7},{6,4},{7,5},{8,10},{9,11},{10,... | collective-permute-start | bytes 1572872 | tf_op jit(solution)/shard_map/ppermute | solution.py:465
  223.4 23.0 %collective-permute-start.19 = (bf16[128,2048]{1,0:T(8,128)(2,1)}, bf16[128,2048]{1,0:T(8,128)(2,1)}, u32[]{:S(2)}, u32[]{:S(2)}) collective-permute-start(bf16[128,2048]{1,0:T(8,128)(2,1)} %get-tuple-element.35), channel_id=1, source_target_pairs={{0,3},{1,0},{2,1},{3,2},{4,7},{5,4},{6,5},{7,6},{8,11},{9,8},{10,9... | collective-permute-start | bytes 1572872 | tf_op jit(solution)/shard_map/ppermute | solution.py:465
  226.8 12.1 %copy-start.32 = (f32[128,2]{0,1:T(2,128)S(1)}, f32[128,2]{0,1:T(2,128)}, u32[]{:S(2)}) copy-start(f32[128,2]{0,1:T(2,128)} %param.35) | copy-start | bytes 3076
  235.6 34.2 %copy-start.28 = (bf16[128,2048]{1,0:T(8,128)(2,1)S(1)}, bf16[128,2048]{1,0:T(8,128)(2,1)}, u32[]{:S(2)}) copy-start(bf16[128,2048]{1,0:T(8,128)(2,1)} %get-tuple-element.23) | copy-start | bytes 1572868
  235.6 24.2 %collective-permute-start.2 = (bf16[128,2048]{1,0:T(8,128)(2,1)}, bf16[128,2048]{1,0:T(8,128)(2,1)}, u32[]{:S(2)}, u32[]{:S(2)}) collective-permute-start(bf16[128,2048]{1,0:T(8,128)(2,1)} %get-tuple-element.26), channel_id=1, source_target_pairs={{0,3},{1,0},{2,1},{3,2},{4,7},{5,4},{6,5},{7,6},{8,11},{9,8},{10,9... | collective-permute-start | bytes 1572872 | tf_op jit(solution)/shard_map/ppermute | solution.py:465
  236.2 23.5 %collective-permute-start.1 = (bf16[128,2048]{1,0:T(8,128)(2,1)}, bf16[128,2048]{1,0:T(8,128)(2,1)}, u32[]{:S(2)}, u32[]{:S(2)}) collective-permute-start(bf16[128,2048]{1,0:T(8,128)(2,1)} %get-tuple-element.25), channel_id=1, source_target_pairs={{0,2},{1,3},{2,0},{3,1},{4,6},{5,7},{6,4},{7,5},{8,10},{9,11},{10,... | collective-permute-start | bytes 1572872 | tf_op jit(solution)/shard_map/ppermute | solution.py:465
  238.8 7.6 %copy-start.26 = (bf16[128,2048]{1,0:T(8,128)(2,1)}, bf16[128,2048]{1,0:T(8,128)(2,1)S(1)}, u32[]{:S(2)}) copy-start(bf16[128,2048]{1,0:T(8,128)(2,1)S(1)} %collective-permute-done.17.refs_3_) | copy-start | bytes 1572868
  238.8 30.9 %collective-permute-start = (bf16[128,2048]{1,0:T(8,128)(2,1)}, bf16[128,2048]{1,0:T(8,128)(2,1)}, u32[]{:S(2)}, u32[]{:S(2)}) collective-permute-start(bf16[128,2048]{1,0:T(8,128)(2,1)} %get-tuple-element.24), channel_id=1, source_target_pairs={{0,1},{1,2},{2,3},{3,0},{4,5},{5,6},{6,7},{7,4},{8,9},{9,10},{10,1... | collective-permute-start | bytes 1572872 | tf_op jit(solution)/shard_map/ppermute | solution.py:465
  244.1 2.3 copy-start.27
  272.2 1.2 copy-start.22
  (8 other events, 7.4 us)
Sparse Core Ops, SparseCore 0:
  66.5 87.9 all-gather.2
